TPU v7x, 32 devices: a whole 2x2x4 slice. The times are simulated.
32 devices in a mesh: grp: 2 (over y), sp: 4 (over z), tp: 4 (over x, core).
Axes of the slice: x: 2, y: 2, z: 4, core: 2. Of those that a mesh axis runs over, the one named last changes fastest.
Arguments:
- tokens: bfloat16 [256, 8, 2048], P(('sp', 'tp'), 'grp'), parts along dimension 1, may hold values from -6 to 6
- norm_gain: float32 [2048], replicated, may hold values from 0.1 to 1.9
- w_query: bfloat16 [2048, 2048], P('sp', 'tp'), may hold values from -0.125 to 0.125
- w_value: bfloat16 [2048, 2048], P('sp', 'tp'), may hold values from -0.125 to 0.125
- w_fwd_gate: bfloat16 [2048, 2048], P('sp', 'tp'), may hold values from -0.125 to 0.125
- w_bwd_gate: bfloat16 [2048, 2048], P('sp', 'tp'), may hold values from -0.125 to 0.125
- w_out_gate: bfloat16 [2048, 2048], P('sp', 'tp'), may hold values from -0.125 to 0.125
- floor_gap: float32 [2, 2048], P(None, 'tp'), may hold values from 0.00078125 to 0.1
- decay_shift: float32 [256, 8, 2048], P('sp', 'grp', 'tp'), parts along dimension 1, may hold values from -1.1 to 0
- head_gain: float32 [128], replicated, may hold values from 0.1 to 1.9
- w_out: bfloat16 [2048, 2048], P('tp', 'sp'), may hold values from -0.125 to 0.125
Outputs:
- layer_out: bfloat16 [256, 8, 2048], P(('sp', 'tp'), 'grp'), parts along dimension 1
There are 2 independent parts, one for each index of `grp`. A program takes and returns all parts, laid end to end along the dimension named above; an argument that names none is the same for every part. Nothing has to cross between parts.
All inputs are finite; a program needn't handle non-finite values.
Results may differ from a plain program's by a relative error of at most 0.013.
Values may be sent and summed in bfloat16 or wider, within the bound.
A program may use at most 128 MiB of HBM per device.

v0:
```python
import jax
import jax.numpy as jnp
from jax import lax
from jax.sharding import PartitionSpec as P

KEY = 128
VAL = 128
BLOCK = 64


norm_eps = 1e-06
highest = lax.Precision.HIGHEST


def carried_in(x, axis, join, neutral, backward):
    count = lax.axis_size(axis)
    place = lax.axis_index(axis)
    ahead = count - 1 - place if backward else place
    gathered = jax.tree.map(
        lambda a, kind: lax.all_gather(a.astype(kind), axis), x, (jnp.bfloat16, jnp.bfloat16)
    )
    state = jax.tree.map(lambda a, e: jnp.zeros_like(a) + jnp.asarray(e, a.dtype), x, neutral)

    def one(turn, state):
        source = count - 1 - turn if backward else turn
        return join(
            state,
            jax.tree.map(
                lambda a, own: lax.dynamic_index_in_dim(a, source, 0, False).astype(own.dtype),
                gathered,
                x,
            ),
        )

    return lax.fori_loop(0, ahead, one, state)


def split_blocks(array):
    return array.reshape(array.shape[0] // BLOCK, BLOCK, *array.shape[1:])


def prepare_chain(queries, key_cols, values, log_decay):
    query_blocks = split_blocks(queries)
    key_blocks = split_blocks(key_cols)
    value_blocks = split_blocks(values)
    running = jnp.cumsum(split_blocks(log_decay), axis=1)
    block_end = running[:, -1]
    block_state = jnp.einsum(
        "nsbhk,nsbhe->nbhke",
        key_blocks * jnp.exp(block_end[:, None] - running),
        value_blocks,
        precision=highest,
    )
    carry_state = jnp.zeros_like(block_state[0])
    log_total = jnp.zeros_like(block_end[0])
    offsets = [log_total]
    carry_state = jnp.exp(block_end[0])[..., None] * carry_state + block_state[0]
    log_total = block_end[0]
    return (
        query_blocks,
        key_blocks,
        value_blocks,
        running,
        block_state,
        jnp.stack(offsets),
        log_total,
        carry_state,
    )


def local_pass(chain, carry_state):
    query_blocks, key_blocks, value_blocks, running, block_state = (
        chain[0],
        chain[1],
        chain[2],
        chain[3],
        chain[4],
    )
    block_len = running.shape[1]
    earlier_mask = jnp.arange(block_len)[:, None] >= jnp.arange(block_len)[None, :]
    here = running[0]
    anchor = here[:1]
    query_scaled = query_blocks[0] * jnp.exp(here - anchor)
    key_scaled = key_blocks[0] * jnp.exp(anchor - here)
    scores = jnp.einsum("tbhk,sbhk->bhts", query_scaled, key_scaled, precision=highest)
    scores = jnp.where(earlier_mask, scores, 0.0)
    within = jnp.einsum("bhts,sbhe->tbhe", scores, value_blocks[0], precision=highest)
    carried = jnp.einsum(
        "tbhk,bhke->tbhe", query_blocks[0] * jnp.exp(here), carry_state, precision=highest
    )
    outputs = within + carried
    return outputs


def combine(earlier, later):
    return (earlier[0] + later[0], jnp.exp(later[0])[..., None] * earlier[1] + later[1])


def group_sums(flat_mixed, weight_lines, group_count):
    group_width = flat_mixed.shape[1] // group_count
    accumulated_total = jnp.zeros((flat_mixed.shape[0], weight_lines.shape[1]), jnp.float32)
    for tp_group in range(group_count):
        first_column = tp_group * group_width
        partial_value = jnp.dot(
            flat_mixed[:, first_column : first_column + group_width],
            weight_lines[first_column : first_column + group_width],
            preferred_element_type=jnp.float32,
        ).astype(jnp.bfloat16)
        accumulated_total = accumulated_total + lax.optimization_barrier(partial_value).astype(
            jnp.float32
        )
    return accumulated_total


def shards(
    tokens,
    norm_gain,
    w_query,
    w_value,
    w_fwd_gate,
    w_bwd_gate,
    w_out_gate,
    floor_gap,
    decay_shift,
    head_gain,
    w_out,
):
    token_f32 = tokens.astype(jnp.float32)
    scale_rows = lax.rsqrt(jnp.mean(token_f32 * token_f32, axis=-1, keepdims=True) + norm_eps)
    normed = (token_f32 * scale_rows * norm_gain).astype(jnp.bfloat16)
    weights = (
        lax.all_gather(w_query, "sp", axis=0, tiled=True),
        lax.all_gather(w_value, "sp", axis=0, tiled=True),
        lax.all_gather(w_fwd_gate, "sp", axis=0, tiled=True),
        lax.all_gather(w_bwd_gate, "sp", axis=0, tiled=True),
        lax.all_gather(w_out_gate, "sp", axis=0, tiled=True),
    )
    piece_rows = lax.all_gather(normed, "tp", axis=0, tiled=True)
    flat_rows = piece_rows.reshape(-1, piece_rows.shape[2])
    columns = [
        jnp.dot(flat_rows, matrix, preferred_element_type=jnp.float32).astype(jnp.bfloat16)
        for matrix in weights
    ]
    projected = lax.optimization_barrier(
        jnp.concatenate(columns, axis=1).reshape(piece_rows.shape[0], piece_rows.shape[1], -1)
    )
    key_width = w_query.shape[1]
    value_width = w_value.shape[1]
    heads_here = key_width // KEY
    extent_rows = projected.shape[0]
    seq_count = projected.shape[1]
    bounds_list = [
        0,
        key_width,
        key_width + value_width,
        2 * key_width + value_width,
        3 * key_width + value_width,
        3 * key_width + 2 * value_width,
    ]

    def section_part(position, feature_lanes):
        picked = projected[:, :, bounds_list[position] : bounds_list[position + 1]].astype(
            jnp.float32
        )
        return picked.reshape(extent_rows, seq_count, heads_here, feature_lanes)

    queries = jax.nn.silu(section_part(0, KEY))
    values = section_part(1, VAL)
    shift = decay_shift.reshape(extent_rows, seq_count, heads_here, KEY)
    key_fwd = floor_gap[0].reshape(heads_here, KEY) * jax.nn.sigmoid(-section_part(2, KEY))
    key_bwd = floor_gap[1].reshape(heads_here, KEY) * jax.nn.sigmoid(-section_part(3, KEY))
    decay_fwd = jnp.log1p(-key_fwd) + shift
    decay_bwd = jnp.log1p(-key_bwd) + shift
    fwd_chain = prepare_chain(queries, key_fwd, values, decay_fwd)
    bwd_chain = prepare_chain(queries[::-1], key_bwd[::-1], values[::-1], decay_bwd[::-1])
    identity_pair = (jnp.zeros_like(fwd_chain[6]), jnp.zeros_like(fwd_chain[7]))
    fwd_in = carried_in((fwd_chain[6], fwd_chain[7]), "sp", combine, identity_pair, False)[1]
    bwd_in = carried_in((bwd_chain[6], bwd_chain[7]), "sp", combine, identity_pair, True)[1]
    out_fwd = local_pass(fwd_chain, fwd_in)
    out_bwd = local_pass(bwd_chain, bwd_in)
    combined = out_fwd + out_bwd[::-1]
    head_normed = (
        combined
        * lax.rsqrt(jnp.mean(combined * combined, axis=-1, keepdims=True) + norm_eps)
        * head_gain
    )
    gate_value = jax.nn.silu(projected[:, :, bounds_list[4] : bounds_list[5]].astype(jnp.float32))
    mixed = (head_normed.reshape(extent_rows, seq_count, value_width) * gate_value).astype(
        jnp.bfloat16
    )
    token_rows = lax.all_to_all(mixed, "tp", split_axis=0, concat_axis=2, tiled=True)
    flat_mixed = token_rows.reshape(-1, token_rows.shape[2])
    group_count = lax.axis_size("tp")
    w_columns = lax.all_gather(w_out, "sp", axis=1, tiled=True)
    w_full = lax.all_gather(w_columns, "tp", axis=0, tiled=True)
    accumulated_total = group_sums(flat_mixed, w_full, group_count)
    result = accumulated_total.reshape(token_rows.shape[0], token_rows.shape[1], -1)
    return result.astype(jnp.bfloat16)


def solution(mesh):
    return jax.shard_map(
        shards,
        mesh=mesh,
        in_specs=(
            P(("sp", "tp"), "grp", None),
            P(),
            P("sp", "tp"),
            P("sp", "tp"),
            P("sp", "tp"),
            P("sp", "tp"),
            P("sp", "tp"),
            P(None, "tp"),
            P("sp", "grp", "tp"),
            P(),
            P("tp", "sp"),
        ),
        out_specs=P(("sp", "tp"), "grp", None),
        check_vma=False,
    )
```

profile of v0, /device:TPU:25, one launch (start us, length us, event | category | flops | bytes accessed | tf_op | source)
XLA Modules:
  0.0 473.5 jit_solution(7733809750445567502)
XLA Ops:
  7.8 1.9 fusion.16
  15.1 12.7 %all-gather.15.cloned.1.call-done = bf16[64,4,2048]{2,1,0:T(4,128)(2,1)} async-done(((bf16[16,4,2048]{2,1,0:T(4,128)(2,1)}), bf16[64,4,2048]{2,1,0:T(4,128)(2,1)}) %all-gather.15.cloned.1.call-update) | async-done | bytes 1048592 | tf_op jit(solution)/shard_map/all_gather | solution.py:138
  29.2 43.8 %all-gather.17.cloned.1.call-done = bf16[2048,512]{1,0:T(8,128)(2,1)} async-done(((bf16[512,512]{1,0:T(8,128)(2,1)}), bf16[2048,512]{1,0:T(8,128)(2,1)}) %all-gather.17.cloned.1.call-update) | async-done | bytes 2097168 | tf_op jit(solution)/shard_map/all_gather | solution.py:132
  73.0 3.0 fusion.9
  76.0 43.0 %all-gather.19.cloned.1.call-done = bf16[2048,512]{1,0:T(8,128)(2,1)} async-done(((bf16[512,512]{1,0:T(8,128)(2,1)}), bf16[2048,512]{1,0:T(8,128)(2,1)}) %all-gather.19.cloned.1.call-update) | async-done | bytes 2097168 | tf_op jit(solution)/shard_map/all_gather | solution.py:133
  119.0 3.0 fusion.10
  122.1 42.9 %all-gather.21.cloned.1.call-done = bf16[2048,512]{1,0:T(8,128)(2,1)} async-done(((bf16[512,512]{1,0:T(8,128)(2,1)}), bf16[2048,512]{1,0:T(8,128)(2,1)}) %all-gather.21.cloned.1.call-update) | async-done | bytes 2097168 | tf_op jit(solution)/shard_map/all_gather | solution.py:134
  165.0 3.0 fusion.11
  168.0 42.9 %all-gather.23.cloned.1.call-done = bf16[2048,512]{1,0:T(8,128)(2,1)} async-done(((bf16[512,512]{1,0:T(8,128)(2,1)}), bf16[2048,512]{1,0:T(8,128)(2,1)}) %all-gather.23.cloned.1.call-update) | async-done | bytes 2097168 | tf_op jit(solution)/shard_map/all_gather | solution.py:135
  210.9 3.0 fusion.12
  213.9 42.9 %all-gather.25.cloned.1.call-done = bf16[2048,512]{1,0:T(8,128)(2,1)} async-done(((bf16[512,512]{1,0:T(8,128)(2,1)}), bf16[2048,512]{1,0:T(8,128)(2,1)}) %all-gather.25.cloned.1.call-update) | async-done | bytes 2097168 | tf_op jit(solution)/shard_map/all_gather | solution.py:136
  256.8 3.0 fusion.13
  259.8 2.6 reshape.198
  267.8 3.0 fusion.36
  272.4 2.8 fusion.5
  276.5 2.5 fusion.35
  278.9 2.0 fusion.4
  281.0 21.8 %all-gather.27.cloned.1.call-done = bf16[512,2048]{1,0:T(8,128)(2,1)} async-done(((bf16[512,512]{1,0:T(8,128)(2,1)}), bf16[512,2048]{1,0:T(8,128)(2,1)}) %all-gather.27.cloned.1.call-update) | async-done | bytes 2097168 | tf_op jit(solution)/shard_map/all_gather | solution.py:194
  302.9 10.5 %all-gather = bf16[4,1,4,4,128]{4,3,2,1,0:T(4,128)(2,1)S(1)} all-gather(bf16[1,1,4,4,128]{4,3,2,1,0:T(4,128)(2,1)S(1)} %slice.123), channel_id=2, replica_groups=mesh['grp'=2,'sp'=4,'tp'=4] {'sp'}, dimensions={0}, use_global_device_ids=true | all-gather | bytes 20480 | tf_op jit(solution)/shard_map/all_gather | solution.py:20
  313.4 10.9 %all-gather.2 = bf16[4,1,4,4,128]{4,3,2,1,0:T(4,128)(2,1)S(1)} all-gather(bf16[1,1,4,4,128]{4,3,2,1,0:T(4,128)(2,1)S(1)} %slice.122), channel_id=4, replica_groups=mesh['grp'=2,'sp'=4,'tp'=4] {'sp'}, dimensions={0}, use_global_device_ids=true | all-gather | bytes 20480 | tf_op jit(solution)/shard_map/all_gather | solution.py:20
  324.2 2.4 convolution_select_fusion.1
  329.7 19.4 %all-gather.33.cloned.1.call-done = bf16[16,4,128,128]{3,2,1,0:T(8,128)(2,1)} async-done(((bf16[4,4,128,128]{3,2,1,0:T(8,128)(2,1)}), bf16[16,4,128,128]{3,2,1,0:T(8,128)(2,1)}) %all-gather.33.cloned.1.call-update) | async-done | bytes 2097168 | tf_op jit(solution)/shard_map/all_gather | solution.py:20
  350.4 44.8 %all-gather.31.cloned.1.call-done = bf16[16,4,128,128]{3,2,1,0:T(8,128)(2,1)} async-done(((bf16[4,4,128,128]{3,2,1,0:T(8,128)(2,1)}), bf16[16,4,128,128]{3,2,1,0:T(8,128)(2,1)}) %all-gather.31.cloned.1.call-update) | async-done | bytes 2097168 | tf_op jit(solution)/shard_map/all_gather | solution.py:20
  395.4 4.9 %while.26 = (s32[]{:T(128)}, f32[4,4,128,128]{3,2,1,0:T(8,128)S(1)}, s32[]{:T(128)}, bf16[4,4,4,128]{3,2,1,0:T(4,128)(2,1)S(1)}, bf16[4,4,4,128,128]{4,3,2,1,0:T(8,128)(2,1)}, /*index=5*/s32[]{:T(128)}, s32[]{:T(128)}, s32[]{:T(128)}) while((s32[]{:T(128)}, f32[4,4,128,128]{3,2,1,0:T(8,128)S(1)}, s32[]{:T(128)}, ...), condition=%wide.region_3.4_spmd, body=%wide.region_2.3_spmd.sunk | while | flops 788485 | bytes 2642047 | solution.py:35
  395.4 1.6 convert_add_fusion.4
  397.1 1.5 convert_add_fusion.4
  402.0 9.5 %all_to_all.15 = bf16[64,4,512]{2,1,0:T(4,128)(2,1)S(1)} all-to-all(bf16[64,4,512]{2,1,0:T(4,128)(2,1)S(1)} %copy.53), channel_id=1, replica_groups=mesh['grp'=2,'sp'=4,'tp'=4] {'tp'}, dimensions={0} | all-to-all | bytes 524288 | tf_op jit(solution)/shard_map/all_to_all | solution.py:191
  411.8 45.6 %all-gather.29.cloned.1.call-done = bf16[2048,2048]{1,0:T(8,128)(2,1)} async-done(((bf16[512,2048]{1,0:T(8,128)(2,1)}), bf16[2048,2048]{1,0:T(8,128)(2,1)}) %all-gather.29.cloned.1.call-update) | async-done | bytes 8388624 | tf_op jit(solution)/shard_map/all_gather | solution.py:195
  457.4 2.1 convolution_convert_fusion.3
  459.5 2.1 convolution_convert_fusion.2
  461.5 2.1 convolution_convert_fusion.1
  463.6 2.1 convolution_convert_fusion
  (85 shorter events, 24.9 us)
Async XLA Ops:
  6.5 7.2 %copy-start.3 = (f32[64,4,512]{2,1,0:T(4,128)S(1)}, f32[64,4,512]{2,1,0:T(4,128)}, u32[]{:S(2)}) copy-start(f32[64,4,512]{2,1,0:T(4,128)} %param.23) | copy-start | bytes 1572868
  6.5 21.3 %all-gather.15.cloned.1.call-start = ((), (), s32[]{:S(2)}) async-start(), calls=%async_computation.1 | async-start | bytes 1310720 | tf_op jit(solution)/shard_map/all_gather | solution.py:138
  9.7 63.3 %all-gather.17.cloned.1.call-start = ((), (), s32[]{:S(2)}) async-start(), calls=%async_computation.2 | async-start | bytes 2621440 | tf_op jit(solution)/shard_map/all_gather | solution.py:132
  10.4 108.6 %all-gather.19.cloned.1.call-start = ((), (), s32[]{:S(2)}) async-start(), calls=%async_computation.3 | async-start | bytes 2621440 | tf_op jit(solution)/shard_map/all_gather | solution.py:133
  11.1 4.0 copy-start.7
  11.2 153.8 %all-gather.21.cloned.1.call-start = ((), (), s32[]{:S(2)}) async-start(), calls=%async_computation.4 | async-start | bytes 2621440 | tf_op jit(solution)/shard_map/all_gather | solution.py:134
  11.7 199.1 %all-gather.23.cloned.1.call-start = ((), (), s32[]{:S(2)}) async-start(), calls=%async_computation.5 | async-start | bytes 2621440 | tf_op jit(solution)/shard_map/all_gather | solution.py:135
  12.3 244.5 %all-gather.25.cloned.1.call-start = ((), (), s32[]{:S(2)}) async-start(), calls=%async_computation.6 | async-start | bytes 2621440 | tf_op jit(solution)/shard_map/all_gather | solution.py:136
  12.9 290.0 %all-gather.27.cloned.1.call-start = ((), (), s32[]{:S(2)}) async-start(), calls=%async_computation.7 | async-start | bytes 2621440 | tf_op jit(solution)/shard_map/all_gather | solution.py:194
  13.6 335.5 %all-gather.33.cloned.1.call-start = ((), (), s32[]{:S(2)}) async-start(), calls=%async_computation.10 | async-start | bytes 2621440 | tf_op jit(solution)/shard_map/all_gather | solution.py:20
  267.7 3.2 copy-start.2
  275.2 120.0 %all-gather.31.cloned.1.call-start = ((), (), s32[]{:S(2)}) async-start(), calls=%async_computation.9 | async-start | bytes 2621440 | tf_op jit(solution)/shard_map/all_gather | solution.py:20
  281.0 176.4 %all-gather.29.cloned.1.call-start = ((), (), s32[]{:S(2)}) async-start(), calls=%async_computation.8 | async-start | bytes 10485760 | tf_op jit(solution)/shard_map/all_gather | solution.py:195
  302.9 25.0 %copy-start = (f32[64,4,4,128]{3,2,1,0:T(4,128)S(1)}, f32[64,4,4,128]{3,2,1,0:T(4,128)}, u32[]{:S(2)}) copy-start(f32[64,4,4,128]{3,2,1,0:T(4,128)} %get-tuple-element.169) | copy-start | bytes 1572868
  302.9 25.0 %copy-start.1 = (f32[64,4,4,128]{3,2,1,0:T(4,128)S(1)}, f32[64,4,4,128]{3,2,1,0:T(4,128)}, u32[]{:S(2)}) copy-start(f32[64,4,4,128]{3,2,1,0:T(4,128)} %get-tuple-element.170) | copy-start | bytes 1572868
  395.4 4.9 %copy-start.4 = (f32[4,4,128,64]{2,3,1,0:T(8,128)S(1)}, f32[4,4,128,64]{2,3,1,0:T(8,128)}, u32[]{:S(2)}) copy-start(f32[4,4,128,64]{2,3,1,0:T(8,128)} %fusion.56) | copy-start | bytes 1572868
  395.4 4.9 %copy-start.5 = (f32[64,4,4,128]{3,2,1,0:T(4,128)S(1)}, f32[64,4,4,128]{3,2,1,0:T(4,128)}, u32[]{:S(2)}) copy-start(f32[64,4,4,128]{3,2,1,0:T(4,128)} %get-tuple-element.155) | copy-start | bytes 1572868
  400.3 1.3 copy-start.6
  400.3 1.3 copy-start.8
Sparse Core Ops, SparseCore 0:
  9.8 18.0 all-gather.14
  29.4 43.4 all-gather.16
  74.5 44.4 all-gather.18
  120.5 44.4 all-gather.20
  166.4 44.4 all-gather.22
  212.3 44.4 all-gather.24
  258.4 44.4 all-gather.26
  304.4 44.6 all-gather.32
  350.7 44.5 all-gather.30
  396.7 60.6 all-gather.28
where the time goes:
time: 474 us; the launch traced here: 473 us
  waiting for transfers between devices  364 us (77%)
  matrix products  36.1 us (8%)
  blocking collectives  30.8 us (6%)
  other arithmetic  18.1 us (4%)
  between operations  13.9 us (3%)
  local copies, waits for them, and re-layouts  10.4 us (2%)
    all_gather x2, waiting for transfers between devices, carried_in(): lax.all_gather(a.astype(kind), axis)  64.2 us
    all_gather x1, waiting for transfers between devices, shards(): w_full = lax.all_gather(w_columns, 'tp', axis=0, tiled=True)  45.6 us
    all_gather x1, waiting for transfers between devices, shards(): lax.all_gather(w_query, 'sp', axis=0, tiled=True)  43.8 us
    all_gather x1, waiting for transfers between devices, shards(): lax.all_gather(w_value, 'sp', axis=0, tiled=True)  43 us
    all_gather x1, waiting for transfers between devices, shards(): lax.all_gather(w_out_gate, 'sp', axis=0, tiled=True)  42.9 us
    all_gather x1, waiting for transfers between devices, shards(): lax.all_gather(w_bwd_gate, 'sp', axis=0, tiled=True)  42.9 us
    all_gather x1, waiting for transfers between devices, shards(): lax.all_gather(w_fwd_gate, 'sp', axis=0, tiled=True)  42.9 us
    all_gather x1, waiting for transfers between devices, shards(): w_columns = lax.all_gather(w_out, 'sp', axis=1, tiled=True)  21.8 us
  transfers between devices with their start and end apart: 10, of which 10 were waited for; matrix products, arithmetic and copies ran while one was open for 11% of the time, Pallas kernels for 0%

commit v1 on v0

--- a/solution.py
+++ b/solution.py
@@ -1,6 +1,10 @@
+import functools
+
 import jax
 import jax.numpy as jnp
 from jax import lax
+from jax.experimental import pallas as pl
+from jax.experimental.pallas import tpu as pltpu
 from jax.sharding import PartitionSpec as P
 
 KEY = 128
@@ -198,9 +202,439 @@
     return result.astype(jnp.bfloat16)
 
 
-def solution(mesh):
+MESH = pl.DeviceIdType.MESH
+CORES = 2
+
+
+def greet(peers):
+    barrier = pltpu.get_barrier_semaphore()
+    for peer in peers:
+        pl.semaphore_signal(barrier, inc=1, device_id=peer, device_id_type=MESH)
+    pl.semaphore_wait(barrier, len(peers))
+
+
+def gather_kernel(
+    sizes,
+    xn_ref,
+    shift_ref,
+    wq_ref,
+    wv_ref,
+    wf_ref,
+    wb_ref,
+    wg_ref,
+    proj_ref,
+    shift_out_ref,
+    acts,
+    weights,
+    shifts,
+    own_sem,
+    az_sem,
+    ax_sem,
+    ac_sem,
+    wz_sem,
+    wy_sem,
+    sz_sem,
+):
+    n_grp, n_sp, n_tp = sizes
+    n_x = n_tp // CORES
+    g = lax.axis_index("grp")
+    s = lax.axis_index("sp")
+    t = lax.axis_index("tp")
+    x = t // CORES
+    c = t % CORES
+    seqs, span = xn_ref.shape[0], xn_ref.shape[1]
+    depth = wq_ref.shape[0]
+    part = depth // n_grp
+    positions = shift_ref.shape[1]
+    sources = (wq_ref, wv_ref, wf_ref, wb_ref, wg_ref)
+
+    z_at = [s] + [lax.rem(s + k, n_sp) for k in range(1, n_sp)]
+    z_from = [s] + [lax.rem(s + n_sp - k, n_sp) for k in range(1, n_sp)]
+    x_at = [t] + [lax.rem(x + j, n_x) * CORES + c for j in range(1, n_x)]
+    x_from = [t] + [lax.rem(x + n_x - j, n_x) * CORES + c for j in range(1, n_x)]
+    twin = x * CORES + (1 - c)
+    y_at = [g] + [lax.rem(g + m, n_grp) for m in range(1, n_grp)]
+    y_from = [g] + [lax.rem(g + n_grp - m, n_grp) for m in range(1, n_grp)]
+
+    peers = [(g, z_at[k], t) for k in range(1, n_sp)]
+    peers += [(g, s, x_at[j]) for j in range(1, n_x)]
+    peers += [(g, s, twin)]
+    peers += [(y_at[m], s, t) for m in range(1, n_grp)]
+    greet(peers)
+
+    def block(where_s, where_t):
+        return acts.at[:, pl.ds(pl.multiple_of((where_s * n_tp + where_t) * span, span), span), :]
+
+    def remote(src, dst, sems, index, peer):
+        return pltpu.make_async_remote_copy(
+            src_ref=src,
+            dst_ref=dst,
+            send_sem=sems.at[(0, *index)],
+            recv_sem=sems.at[(1, *index)],
+            device_id=peer,
+            device_id_type=MESH,
+        )
+
+    def rows(where_s, where_g):
+        return pl.ds(pl.multiple_of(where_s * depth + where_g * part, part), part)
+
+    def lanes(where):
+        return pl.ds(pl.multiple_of(where * KEY, KEY), KEY)
+
+    mine = [
+        pltpu.make_async_copy(
+            w.at[:, lanes(s)],
+            weights.at[pl.ds(pl.multiple_of(s * depth, depth), depth), pl.ds(p * KEY, KEY)],
+            own_sem.at[p],
+        )
+        for p, w in enumerate(sources)
+    ]
+    mine.append(pltpu.make_async_copy(xn_ref, block(s, t), own_sem.at[len(sources)]))
+    mine.append(
+        pltpu.make_async_copy(
+            shift_ref.at[:, :, lanes(s)],
+            shifts.at[:, pl.ds(pl.multiple_of(s * positions, positions), positions), :],
+            own_sem.at[len(sources) + 1],
+        )
+    )
+
+    sent = []
+
+    def go(copy):
+        copy.start()
+        sent.append(copy)
+        return copy
+
+    act_z = {}
+    act_x = {}
+    for k in range(1, n_sp):
+        act_z[k] = go(remote(xn_ref, block(s, t), az_sem, (k - 1,), (g, z_at[k], t)))
+    for j in range(1, n_x):
+        act_x[j, 0] = go(remote(xn_ref, block(s, t), ax_sem, (j - 1, 0), (g, s, x_at[j])))
+    act_c = {}
+    act_c[0, 0] = go(remote(xn_ref, block(s, t), ac_sem, (0, 0), (g, s, twin)))
+    w_z = {}
+    for k in range(1, n_sp):
+        for p, w in enumerate(sources):
+            w_z[k, p] = go(
+                remote(
+                    w.at[pl.ds(pl.multiple_of(g * part, part), part), lanes(z_at[k])],
+                    weights.at[rows(s, g), pl.ds(p * KEY, KEY)],
+                    wz_sem,
+                    (k - 1, p),
+                    (g, z_at[k], t),
+                )
+            )
+    s_z = {}
+    for k in range(1, n_sp):
+        s_z[k] = go(
+            remote(
+                shift_ref.at[:, :, lanes(z_at[k])],
+                shifts.at[:, pl.ds(pl.multiple_of(s * positions, positions), positions), :],
+                sz_sem,
+                (k - 1,),
+                (g, z_at[k], t),
+            )
+        )
+    for copy in mine:
+        copy.start()
+
+    for k in range(1, n_sp):
+        act_z[k].wait_recv()
+        here = block(z_from[k], t)
+        for j in range(1, n_x):
+            act_x[j, k] = go(remote(here, here, ax_sem, (j - 1, k), (g, s, x_at[j])))
+        act_c[0, k] = go(remote(here, here, ac_sem, (0, k), (g, s, twin)))
+    for k in range(n_sp):
+        for j in range(1, n_x):
+            act_x[j, k].wait_recv()
+            here = block(z_from[k], x_from[j])
+            act_c[j, k] = go(remote(here, here, ac_sem, (j, k), (g, s, twin)))
+    w_y = {}
+    for k in range(1, n_sp):
+        for p in range(len(sources)):
+            w_z[k, p].wait_recv()
+            here = weights.at[rows(z_from[k], g), pl.ds(p * KEY, KEY)]
+            for m in range(1, n_grp):
+                w_y[m, k, p] = go(remote(here, here, wy_sem, (m - 1, k - 1, p), (y_at[m], s, t)))
+    for copy in mine:
+        copy.wait()
+    for copy in act_c.values():
+        copy.wait_recv()
+    for copy in w_y.values():
+        copy.wait_recv()
+
+    def project(q, carry):
+        proj_ref[q] = jnp.dot(
+            acts[q], weights[...], preferred_element_type=jnp.float32
+        ).astype(jnp.bfloat16)
+        return carry
+
+    lax.fori_loop(0, seqs, project, 0)
+    for copy in s_z.values():
+        copy.wait_recv()
+    shift_out_ref[...] = shifts[...]
+    for copy in sent:
+        copy.wait_send()
+
+
+def gather_project(sizes, xn, shift, sources):
+    n_grp, n_sp, n_tp = sizes
+    n_x = n_tp // CORES
+    seqs, span, model = xn.shape
+    length = n_sp * n_tp * span
+    width = len(sources) * KEY
+    dma = pltpu.SemaphoreType.DMA
+    hbm = pl.BlockSpec(memory_space=pltpu.HBM)
+    vmem = pl.BlockSpec(memory_space=pltpu.VMEM)
+    return pl.pallas_call(
+        functools.partial(gather_kernel, sizes),
+        out_shape=(
+            jax.ShapeDtypeStruct((seqs, length, width), jnp.bfloat16),
+            jax.ShapeDtypeStruct((seqs, length, KEY), jnp.float32),
+        ),
+        in_specs=[hbm] * (2 + len(sources)),
+        out_specs=(vmem, vmem),
+        scratch_shapes=[
+            pltpu.VMEM((seqs, length, model), jnp.bfloat16),
+            pltpu.VMEM((model, width), jnp.bfloat16),
+            pltpu.VMEM((seqs, length, KEY), jnp.float32),
+            dma((len(sources) + 2,)),
+            dma((2, n_sp - 1)),
+            dma((2, max(n_x - 1, 1), n_sp)),
+            dma((2, n_x, n_sp)),
+            dma((2, n_sp - 1, len(sources))),
+            dma((2, max(n_grp - 1, 1), n_sp - 1, len(sources))),
+            dma((2, n_sp - 1)),
+        ],
+        compiler_params=pltpu.CompilerParams(
+            collective_id=0, has_side_effects=True, vmem_limit_bytes=56 * 1024 * 1024
+        ),
+    )(xn, shift, *sources)
+
+
+def recur_kernel(proj_ref, shift_ref, gap_ref, gain_ref, mixed_ref, out_ref):
+    f32 = jnp.float32
+    bf16 = jnp.bfloat16
+    length = proj_ref.shape[1]
+
+    def cols(p):
+        return proj_ref[0, :, p * KEY : (p + 1) * KEY]
+
+    queries = cols(0).astype(f32)
+    queries = queries * jax.nn.sigmoid(queries)
+    values = cols(1)
+    shift = shift_ref[0]
+    row = lax.broadcasted_iota(jnp.int32, (BLOCK, BLOCK), 0)
+    col = lax.broadcasted_iota(jnp.int32, (BLOCK, BLOCK), 1)
+    blocks = length // BLOCK
+    for d in range(2):
+        keys = gap_ref[d : d + 1, :] * jax.nn.sigmoid(-cols(2 + d).astype(f32))
+        decay = jnp.log1p(-keys) + shift
+        seen = (row >= col) if d == 0 else (row <= col)
+        tri = jnp.where(seen, 1.0, 0.0).astype(f32)
+        state = None
+        for step in range(blocks):
+            n = step if d == 0 else blocks - 1 - step
+            at = slice(n * BLOCK, (n + 1) * BLOCK)
+            q, k, v = queries[at], keys[at], values[at]
+            here = jnp.dot(tri, decay[at], precision=highest, preferred_element_type=f32)
+            edge = here[BLOCK - 1 : BLOCK] if d == 0 else here[0:1]
+            anchor = here[BLOCK // 2 : BLOCK // 2 + 1]
+            scores = lax.dot_general(
+                (q * jnp.exp(here - anchor)).astype(bf16),
+                (k * jnp.exp(anchor - here)).astype(bf16),
+                (((1,), (1,)), ((), ())),
+                preferred_element_type=f32,
+            )
+            scores = jnp.where(seen, scores, 0.0).astype(bf16)
+            out = jnp.dot(scores, v, preferred_element_type=f32)
+            if state is not None:
+                out = out + lax.dot_general(
+                    (q * jnp.exp(here)).astype(bf16),
+                    state.astype(bf16),
+                    (((1,), (1,)), ((), ())),
+                    preferred_element_type=f32,
+                )
+            if d == 0:
+                out_ref[at] = out
+            else:
+                out_ref[at] = out_ref[at] + out
+            if step < blocks - 1:
+                fresh = lax.dot_general(
+                    v,
+                    (k * jnp.exp(edge - here)).astype(bf16),
+                    (((0,), (0,)), ((), ())),
+                    preferred_element_type=f32,
+                )
+                state = fresh if state is None else state * jnp.exp(edge) + fresh
+    combined = out_ref[...]
+    normed = combined * lax.rsqrt(jnp.mean(combined * combined, axis=-1, keepdims=True) + norm_eps)
+    gate = cols(4).astype(f32)
+    mixed_ref[0] = (normed * gain_ref[...] * (gate * jax.nn.sigmoid(gate))).astype(bf16)
+
+
+def recur(proj, shift, gap, gain):
+    seqs, length, width = proj.shape
+    return pl.pallas_call(
+        recur_kernel,
+        grid=(seqs,),
+        out_shape=jax.ShapeDtypeStruct((seqs, length, VAL), jnp.bfloat16),
+        in_specs=[
+            pl.BlockSpec((1, length, width), lambda i: (i, 0, 0)),
+            pl.BlockSpec((1, length, KEY), lambda i: (i, 0, 0)),
+            pl.BlockSpec((2, KEY), lambda i: (0, 0)),
+            pl.BlockSpec((1, VAL), lambda i: (0, 0)),
+        ],
+        out_specs=pl.BlockSpec((1, length, VAL), lambda i: (i, 0, 0)),
+        scratch_shapes=[pltpu.VMEM((length, VAL), jnp.float32)],
+    )(proj, shift, gap, gain)
+
+
+def mix_kernel(sizes, mixed_ref, w_ref, out_ref, heads, partial, landed, own_sem, m_sem, p_sem):
+    n_grp, n_sp, n_tp = sizes
+    g = lax.axis_index("grp")
+    s = lax.axis_index("sp")
+    t = lax.axis_index("tp")
+    seqs = mixed_ref.shape[0]
+    span = out_ref.shape[1]
+    width = w_ref.shape[1]
+    z_at = [lax.rem(s + k, n_sp) for k in range(n_sp)]
+    z_from = [lax.rem(s + n_sp - k, n_sp) for k in range(n_sp)]
+    t_at = [lax.rem(t + j, n_tp) for j in range(n_tp)]
+    t_from = [lax.rem(t + n_tp - j, n_tp) for j in range(n_tp)]
+    others = [(k, j) for k in range(n_sp) for j in range(n_tp) if k or j]
+    greet([(g, z_at[k], t_at[j]) for k, j in others])
+
+    def lanes(where, size):
+        return pl.ds(pl.multiple_of(where * size, size), size)
+
+    own = pltpu.make_async_copy(mixed_ref, heads.at[:, :, lanes(s, VAL)], own_sem)
+    own.start()
+    moves = [
+        pltpu.make_async_remote_copy(
+            src_ref=mixed_ref,
+            dst_ref=heads.at[:, :, lanes(s, VAL)],
+            send_sem=m_sem.at[0, k - 1],
+            recv_sem=m_sem.at[1, k - 1],
+            device_id=(g, z_at[k], t),
+            device_id_type=MESH,
+        )
+        for k in range(1, n_sp)
+    ]
+    for copy in moves:
+        copy.start()
+    own.wait()
+    for copy in moves:
+        copy.wait_recv()
+
+    def multiply(q, carry):
+        partial[q] = jnp.dot(
+            heads[q], w_ref[...], preferred_element_type=jnp.float32
+        ).astype(jnp.bfloat16)
+        return carry
+
+    lax.fori_loop(0, seqs, multiply, 0)
+
+    def piece(where_s, where_t):
+        return pl.ds(pl.multiple_of((where_s * n_tp + where_t) * span, span), span)
+
+    sends = [
+        pltpu.make_async_remote_copy(
+            src_ref=partial.at[:, piece(z_at[k], t_at[j]), :],
+            dst_ref=landed.at[t, :, :, lanes(s, width)],
+            send_sem=p_sem.at[0, k, j],
+            recv_sem=p_sem.at[1, k, j],
+            device_id=(g, z_at[k], t_at[j]),
+            device_id_type=MESH,
+        )
+        for k, j in others
+    ]
+    for copy in sends:
+        copy.start()
+    landed[t, :, :, lanes(s, width)] = partial[:, piece(s, t), :]
+    for copy in sends:
+        copy.wait_recv()
+    total = landed[0].astype(jnp.float32)
+    for j in range(1, n_tp):
+        total = total + landed[j].astype(jnp.float32)
+    out_ref[...] = total.astype(jnp.bfloat16)
+    for copy in moves + sends:
+        copy.wait_send()
+
+
+def mix(sizes, mixed, w_out):
+    n_grp, n_sp, n_tp = sizes
+    seqs, length, _ = mixed.shape
+    span = length // (n_sp * n_tp)
+    depth, width = w_out.shape
+    dma = pltpu.SemaphoreType.DMA
+    vmem = pl.BlockSpec(memory_space=pltpu.VMEM)
+    return pl.pallas_call(
+        functools.partial(mix_kernel, sizes),
+        out_shape=jax.ShapeDtypeStruct((seqs, span, n_sp * width), jnp.bfloat16),
+        in_specs=[pl.BlockSpec(memory_space=pltpu.HBM), vmem],
+        out_specs=vmem,
+        scratch_shapes=[
+            pltpu.VMEM((seqs, length, depth), jnp.bfloat16),
+            pltpu.VMEM((seqs, length, width), jnp.bfloat16),
+            pltpu.VMEM((n_tp, seqs, span, n_sp * width), jnp.bfloat16),
+            dma,
+            dma((2, n_sp - 1)),
+            dma((2, n_sp, n_tp)),
+        ],
+        compiler_params=pltpu.CompilerParams(collective_id=1, has_side_effects=True),
+    )(mixed, w_out)
+
+
+def head_shards(
+    sizes,
+    tokens,
+    norm_gain,
+    w_query,
+    w_value,
+    w_fwd_gate,
+    w_bwd_gate,
+    w_out_gate,
+    floor_gap,
+    decay_shift,
+    head_gain,
+    w_out,
+):
+    token_f32 = tokens.astype(jnp.float32)
+    scale_rows = lax.rsqrt(jnp.mean(token_f32 * token_f32, axis=-1, keepdims=True) + norm_eps)
+    normed = (token_f32 * scale_rows * norm_gain).astype(jnp.bfloat16)
+    proj, shift = gather_project(
+        sizes,
+        normed.transpose(1, 0, 2),
+        decay_shift.transpose(1, 0, 2),
+        (w_query, w_value, w_fwd_gate, w_bwd_gate, w_out_gate),
+    )
+    first = lax.axis_index("sp") * KEY
+    gap = lax.dynamic_slice_in_dim(floor_gap, first, KEY, axis=1)
+    mixed = recur(proj, shift, gap, head_gain.reshape(1, VAL))
+    return mix(sizes, mixed, w_out).transpose(1, 0, 2)
+
+
+def by_heads(mesh):
+    n_sp, n_tp = mesh.shape["sp"], mesh.shape["tp"]
+
+    def run(*arrays):
+        tokens, w_query = arrays[0], arrays[2]
+        heads_here = w_query.shape[1] // KEY // n_tp
+        span = tokens.shape[0] // (n_sp * n_tp)
+        sizes = (mesh.shape["grp"], n_sp, n_tp)
+        fits = heads_here == n_sp and n_sp > 1 and n_tp % CORES == 0 and span % 16 == 0
+        fits = fits and tokens.shape[0] % BLOCK == 0 and tokens.shape[0] <= 512
+        body = functools.partial(head_shards, sizes) if fits else shards
+        return mapped(body, mesh)(*arrays)
+
+    return run
+
+
+def mapped(body, mesh):
     return jax.shard_map(
-        shards,
+        body,
         mesh=mesh,
         in_specs=(
             P(("sp", "tp"), "grp", None),
@@ -218,3 +652,7 @@
         out_specs=P(("sp", "tp"), "grp", None),
         check_vma=False,
     )
+
+
+def solution(mesh):
+    return by_heads(mesh)

time: 474 us -> 151 us (0.32)
  waiting for transfers between devices: 364 us -> 0 us
  Pallas kernels: 0 us -> 143 us
  matrix products: 36.1 us -> 0 us
  blocking collectives: 30.8 us -> 0 us
  other arithmetic: 18.1 us -> 3.11 us
  between operations: 13.9 us -> 0.03 us
  local copies, waits for them, and re-layouts: 10.4 us -> 4.48 us
    all_gather x10 -> x0, waiting for transfers between devices: 360 us -> none  [the longest x2 64.2 us: carried_in(): lax.all_gather(a.astype(kind), axis)]
    pallas_call x0 -> x3, Pallas kernels: none -> 143 us  [the longest x1 76 us: gather_project(): pl.pallas_call(functools.partial(gather_kernel, sizes), out_shape=(jax.Sh...]
    dot_general x17 -> x0, matrix products: 36.1 us -> none  [the longest x5 15.2 us: shards(): jnp.dot(flat_rows, matrix, preferred_element_type=jnp.float32)]
    all_gather x2 -> x0, blocking collectives: 21.3 us -> none  [carried_in(): lax.all_gather(a.astype(kind), axis)]
    all_to_all x1 -> x0, blocking collectives: 9.49 us -> none  [shards(): lax.all_to_all(mixed, 'tp', split_axis=0, concat_axis=2, tiled=True)]
    reshape x5 -> x0, local copies, waits for them, and re-layouts: 6.45 us -> none  [the longest x1 2.61 us: shards(): jnp.concatenate(columns, axis=1)]
    add x4 -> x0, other arithmetic: 5.91 us -> none  [the longest x3 4.71 us: combine(): jnp.exp(later[0])[..., None] * earlier[1] + later[1]]
  transfers between devices with their start and end apart: 10 -> 0, of which waited for: 10 -> 0; matrix products, arithmetic and copies ran while one was open for 11% -> 0% of each run, Pallas kernels for 0% -> 0%
where the time goes in v1:
time: 151 us; the launch traced here: 150 us
  Pallas kernels  143 us (95%)
  local copies, waits for them, and re-layouts  4.48 us (3%)
  other arithmetic  3.11 us (2%)
    pallas_call x1, Pallas kernels, gather_project(): pl.pallas_call(functools.partial(gather_kernel, sizes), out_shape=(jax.Sh...  76 us
    pallas_call x1, Pallas kernels, mix(): pl.pallas_call(functools.partial(mix_kernel, sizes), out_shape=jax.ShapeD...  56.1 us
    pallas_call x1, Pallas kernels, recur(): pl.pallas_call(recur_kernel, grid=(seqs,), out_shape=jax.ShapeDtypeStruct...  10.7 us

profile of v1, /device:TPU:25, one launch (start us, length us, event | category | flops | bytes accessed | tf_op | source)
XLA Modules:
  0.0 150.4 jit_solution(8956715202939735493)
XLA Ops:
  0.0 0.0 copy-start
  0.0 1.2 fusion
  1.2 1.9 %fusion.3.xn_ref = bf16[4,16,2048]{2,1,0:T(8,128)(2,1)} fusion(f32[2048]{0:T(1024)} %param.12, f32[16,4]{0,1:T(4,128)S(1)} %add_rsqrt_fusion, bf16[16,4,2048]{2,1,0:T(4,128)(2,1)} %param.11), kind=kLoop, calls=%fused_computation.6 | loop fusion | flops 524288 | bytes 532736 | tf_op jit(solution)/shard_map/transpose | solution.py:609
  3.1 2.0 %copy.18 = f32[64,4,512]{2,0,1:T(8,128)} copy(f32[64,4,512]{2,1,0:T(4,128)} %param.19) | data formatting | bytes 1048576 | tf_op args[8]
  5.1 76.0 %shard_map.109 = (bf16[4,256,640]{2,1,0:T(8,128)(2,1)}, f32[4,256,128]{2,1,0:T(8,128)}) custom-call(bf16[4,16,2048]{2,1,0:T(8,128)(2,1)} %fusion.3.xn_ref, f32[4,64,512]{2,1,0:T(8,128)} %bitcast.7, bf16[512,512]{1,0:T(8,128)(2,1)} %wq_ref.1, bf16[512,512]{1,0:T(8,128)(2,1)} %wv_ref.1, bf16[512,512]{1,0:T(8,128)(2,1)} %wf_ref.1, bf16[512,512]{1,0:T(8,128)(2,1)} %wb_ref.1, ...), custom_call_target="tpu_custom_call" | custom-call | tf_op jit(solution)/shard_map/pallas_call | solution.py:390
  81.1 0.0 copy-done
  81.2 0.6 constant_dynamic-slice_fusion.gap_ref
  81.8 10.7 %shard_map.110.mixed_ref = bf16[4,256,128]{2,1,0:T(8,128)(2,1)} custom-call(bf16[4,256,640]{2,1,0:T(8,128)(2,1)} %get-tuple-element.7.proj_ref, f32[4,256,128]{2,1,0:T(8,128)} %get-tuple-element.8.shift_ref, f32[2,128]{1,0:T(2,128)} %constant_dynamic-slice_fusion.gap_ref, f32[1,128]{1,0:T(1,128)} %bitcast.9), custom_call_target="tpu_custom_call" | custom-call | tf_op jit(solution)/shard_map/pallas_call | solution.py:479
  92.4 56.1 %shard_map.111 = bf16[4,16,2048]{2,1,0:T(8,128)(2,1)} custom-call(bf16[4,256,128]{2,1,0:T(8,128)(2,1)} %shard_map.110.mixed_ref, bf16[512,512]{1,0:T(8,128)(2,1)} %w_ref.1), custom_call_target="tpu_custom_call" | custom-call | tf_op jit(solution)/shard_map/pallas_call | solution.py:573
  148.6 1.9 %copy.14 = bf16[16,4,2048]{2,1,0:T(4,128)(2,1)} copy(bf16[16,4,2048]{2,0,1:T(8,128)(2,1)} %bitcast.8) | data formatting | bytes 524288 | tf_op jit(solution)/shard_map/transpose | solution.py:616
  (1 shorter events, 0.0 us)
Async XLA Ops:
  0.0 81.2 %copy-start = (f32[2,512]{1,0:T(2,128)S(1)}, f32[2,512]{1,0:T(2,128)}, u32[]{:S(2)}) copy-start(f32[2,512]{1,0:T(2,128)} %param.18) | copy-start | bytes 12292

commit v2 on v1

--- a/solution.py
+++ b/solution.py
@@ -305,26 +305,80 @@
         sent.append(copy)
         return copy
 
-    act_z = {}
-    act_x = {}
-    for k in range(1, n_sp):
-        act_z[k] = go(remote(xn_ref, block(s, t), az_sem, (k - 1,), (g, z_at[k], t)))
+    def slot(up, d):
+        return 1 + d if up else n_sp + d
+
+    def chain(up, d):
+        step = -1 if up else 1
+        there = s - step
+        sends = jnp.logical_and(
+            jnp.logical_and(there >= 0, there < n_sp),
+            jnp.logical_and(s + step * d >= 0, s + step * d < n_sp),
+        )
+        gets = jnp.logical_and(s + step * (d + 1) >= 0, s + step * (d + 1) < n_sp)
+        return there, s + step * d, sends, s + step * (d + 1), gets
+
+    def act_move(up, d, from_own):
+        there, origin, _, _, _ = chain(up, d)
+        src = xn_ref if from_own else block(origin, t)
+        return remote(src, block(origin, t), az_sem, (slot(up, d) - 1,), (g, there, t))
+
+    def act_spread(kind, j, index, where_s, where_t, from_own):
+        src = xn_ref if from_own else block(where_s, where_t)
+        if kind == "x":
+            return remote(src, block(where_s, where_t), ax_sem, (j - 1, index), (g, s, x_at[j]))
+        return remote(src, block(where_s, where_t), ac_sem, (j, index), (g, s, twin))
+
+    for up in (True, False):
+        _, _, sends, _, _ = chain(up, 0)
+
+        @pl.when(sends)
+        def _():
+            act_move(up, 0, True).start()
+
     for j in range(1, n_x):
-        act_x[j, 0] = go(remote(xn_ref, block(s, t), ax_sem, (j - 1, 0), (g, s, x_at[j])))
-    act_c = {}
-    act_c[0, 0] = go(remote(xn_ref, block(s, t), ac_sem, (0, 0), (g, s, twin)))
+        act_spread("x", j, 0, s, t, True).start()
+    act_spread("c", 0, 0, s, t, True).start()
+    for copy in mine:
+        copy.start()
+
     w_z = {}
-    for k in range(1, n_sp):
-        for p, w in enumerate(sources):
+
+    def send_weights(p):
+        for k in range(1, n_sp):
             w_z[k, p] = go(
                 remote(
-                    w.at[pl.ds(pl.multiple_of(g * part, part), part), lanes(z_at[k])],
+                    sources[p].at[pl.ds(pl.multiple_of(g * part, part), part), lanes(z_at[k])],
                     weights.at[rows(s, g), pl.ds(p * KEY, KEY)],
                     wz_sem,
                     (k - 1, p),
                     (g, z_at[k], t),
                 )
             )
+
+    queue = list(range(len(sources)))
+    for d in range(n_sp - 1):
+        if queue:
+            send_weights(queue.pop(0))
+        for up in (True, False):
+            _, _, _, origin, gets = chain(up, d)
+
+            @pl.when(gets)
+            def _():
+                act_move(up, d, False).wait_recv()
+                if d + 1 < n_sp - 1:
+                    _, _, sends, _, _ = chain(up, d + 1)
+
+                    @pl.when(sends)
+                    def _():
+                        act_move(up, d + 1, False).start()
+
+                for j in range(1, n_x):
+                    act_spread("x", j, slot(up, d), origin, t, False).start()
+                act_spread("c", 0, slot(up, d), origin, t, False).start()
+
+    for p in queue:
+        send_weights(p)
     s_z = {}
     for k in range(1, n_sp):
         s_z[k] = go(
@@ -336,44 +390,70 @@
                 (g, z_at[k], t),
             )
         )
-    for copy in mine:
-        copy.start()
-
-    for k in range(1, n_sp):
-        act_z[k].wait_recv()
-        here = block(z_from[k], t)
+
+    def each_block(visit):
+        visit(0, s)
+        for d in range(n_sp - 1):
+            for up in (True, False):
+                _, _, _, origin, gets = chain(up, d)
+
+                @pl.when(gets)
+                def _():
+                    visit(slot(up, d), origin)
+
+    def relay(index, origin):
         for j in range(1, n_x):
-            act_x[j, k] = go(remote(here, here, ax_sem, (j - 1, k), (g, s, x_at[j])))
-        act_c[0, k] = go(remote(here, here, ac_sem, (0, k), (g, s, twin)))
-    for k in range(n_sp):
-        for j in range(1, n_x):
-            act_x[j, k].wait_recv()
-            here = block(z_from[k], x_from[j])
-            act_c[j, k] = go(remote(here, here, ac_sem, (j, k), (g, s, twin)))
+            act_spread("x", j, index, origin, t, False).wait_recv()
+            act_spread("c", j, index, origin, x_from[j], False).start()
+
+    each_block(relay)
     w_y = {}
-    for k in range(1, n_sp):
-        for p in range(len(sources)):
+    for p in range(len(sources)):
+        for k in range(1, n_sp):
             w_z[k, p].wait_recv()
             here = weights.at[rows(z_from[k], g), pl.ds(p * KEY, KEY)]
             for m in range(1, n_grp):
                 w_y[m, k, p] = go(remote(here, here, wy_sem, (m - 1, k - 1, p), (y_at[m], s, t)))
     for copy in mine:
         copy.wait()
-    for copy in act_c.values():
-        copy.wait_recv()
-    for copy in w_y.values():
-        copy.wait_recv()
-
-    def project(q, carry):
-        proj_ref[q] = jnp.dot(
-            acts[q], weights[...], preferred_element_type=jnp.float32
-        ).astype(jnp.bfloat16)
-        return carry
-
-    lax.fori_loop(0, seqs, project, 0)
+
+    def joined(index, origin):
+        for j in range(n_x):
+            act_spread("c", j, index, origin, t, False).wait_recv()
+
+    each_block(joined)
+    for first in range(0, len(sources), 2):
+        last = min(first + 2, len(sources))
+        for (m, k, p), copy in w_y.items():
+            if first <= p < last:
+                copy.wait_recv()
+        at = slice(first * KEY, last * KEY)
+
+        def project(q, carry):
+            proj_ref[q, :, at] = jnp.dot(
+                acts[q], weights[:, at], preferred_element_type=jnp.float32
+            ).astype(jnp.bfloat16)
+            return carry
+
+        lax.fori_loop(0, seqs, project, 0)
     for copy in s_z.values():
         copy.wait_recv()
     shift_out_ref[...] = shifts[...]
+    for d in range(n_sp - 1):
+        for up in (True, False):
+            _, _, sends, _, _ = chain(up, d)
+
+            @pl.when(sends)
+            def _():
+                act_move(up, d, d == 0).wait_send()
+
+    def gone(index, origin):
+        for j in range(1, n_x):
+            act_spread("x", j, index, origin, t, False).wait_send()
+        for j in range(n_x):
+            act_spread("c", j, index, origin, x_from[j], False).wait_send()
+
+    each_block(gone)
     for copy in sent:
         copy.wait_send()
 
@@ -391,18 +471,18 @@
         functools.partial(gather_kernel, sizes),
         out_shape=(
             jax.ShapeDtypeStruct((seqs, length, width), jnp.bfloat16),
-            jax.ShapeDtypeStruct((seqs, length, KEY), jnp.float32),
+            jax.ShapeDtypeStruct((seqs, length, KEY), shift.dtype),
         ),
         in_specs=[hbm] * (2 + len(sources)),
         out_specs=(vmem, vmem),
         scratch_shapes=[
             pltpu.VMEM((seqs, length, model), jnp.bfloat16),
             pltpu.VMEM((model, width), jnp.bfloat16),
-            pltpu.VMEM((seqs, length, KEY), jnp.float32),
+            pltpu.VMEM((seqs, length, KEY), shift.dtype),
             dma((len(sources) + 2,)),
-            dma((2, n_sp - 1)),
-            dma((2, max(n_x - 1, 1), n_sp)),
-            dma((2, n_x, n_sp)),
+            dma((2, 2 * n_sp - 2)),
+            dma((2, max(n_x - 1, 1), 2 * n_sp - 1)),
+            dma((2, n_x, 2 * n_sp - 1)),
             dma((2, n_sp - 1, len(sources))),
             dma((2, max(n_grp - 1, 1), n_sp - 1, len(sources))),
             dma((2, n_sp - 1)),
@@ -413,18 +493,18 @@
     )(xn, shift, *sources)
 
 
-def recur_kernel(proj_ref, shift_ref, gap_ref, gain_ref, mixed_ref, out_ref):
+def recur_one(proj_ref, shift_ref, gap_ref, gain_ref, out_ref, i):
     f32 = jnp.float32
     bf16 = jnp.bfloat16
     length = proj_ref.shape[1]
 
     def cols(p):
-        return proj_ref[0, :, p * KEY : (p + 1) * KEY]
+        return proj_ref[i, :, p * KEY : (p + 1) * KEY]
 
     queries = cols(0).astype(f32)
     queries = queries * jax.nn.sigmoid(queries)
     values = cols(1)
-    shift = shift_ref[0]
+    shift = shift_ref[i].astype(f32)
     row = lax.broadcasted_iota(jnp.int32, (BLOCK, BLOCK), 0)
     col = lax.broadcasted_iota(jnp.int32, (BLOCK, BLOCK), 1)
     blocks = length // BLOCK
@@ -471,120 +551,232 @@
     combined = out_ref[...]
     normed = combined * lax.rsqrt(jnp.mean(combined * combined, axis=-1, keepdims=True) + norm_eps)
     gate = cols(4).astype(f32)
-    mixed_ref[0] = (normed * gain_ref[...] * (gate * jax.nn.sigmoid(gate))).astype(bf16)
-
-
-def recur(proj, shift, gap, gain):
-    seqs, length, width = proj.shape
-    return pl.pallas_call(
-        recur_kernel,
-        grid=(seqs,),
-        out_shape=jax.ShapeDtypeStruct((seqs, length, VAL), jnp.bfloat16),
-        in_specs=[
-            pl.BlockSpec((1, length, width), lambda i: (i, 0, 0)),
-            pl.BlockSpec((1, length, KEY), lambda i: (i, 0, 0)),
-            pl.BlockSpec((2, KEY), lambda i: (0, 0)),
-            pl.BlockSpec((1, VAL), lambda i: (0, 0)),
-        ],
-        out_specs=pl.BlockSpec((1, length, VAL), lambda i: (i, 0, 0)),
-        scratch_shapes=[pltpu.VMEM((length, VAL), jnp.float32)],
-    )(proj, shift, gap, gain)
-
-
-def mix_kernel(sizes, mixed_ref, w_ref, out_ref, heads, partial, landed, own_sem, m_sem, p_sem):
+    return (normed * gain_ref[...] * (gate * jax.nn.sigmoid(gate))).astype(bf16)
+
+
+def mix_kernel(
+    sizes,
+    proj_ref,
+    shift_ref,
+    gap_ref,
+    gain_ref,
+    w_ref,
+    out_ref,
+    summed,
+    heads,
+    matrix,
+    partial,
+    landed,
+    own_sem,
+    w_sem,
+    z_sem,
+    c_sem,
+    p_sem,
+):
     n_grp, n_sp, n_tp = sizes
+    n_x = n_tp // CORES
     g = lax.axis_index("grp")
     s = lax.axis_index("sp")
     t = lax.axis_index("tp")
-    seqs = mixed_ref.shape[0]
+    x = t // CORES
+    c = t % CORES
+    twin = x * CORES + (1 - c)
+    seqs = proj_ref.shape[0]
     span = out_ref.shape[1]
-    width = w_ref.shape[1]
+    depth, width = w_ref.shape[0], w_ref.shape[1] // CORES
+    half = seqs // 2
     z_at = [lax.rem(s + k, n_sp) for k in range(n_sp)]
-    z_from = [lax.rem(s + n_sp - k, n_sp) for k in range(n_sp)]
     t_at = [lax.rem(t + j, n_tp) for j in range(n_tp)]
-    t_from = [lax.rem(t + n_tp - j, n_tp) for j in range(n_tp)]
     others = [(k, j) for k in range(n_sp) for j in range(n_tp) if k or j]
     greet([(g, z_at[k], t_at[j]) for k, j in others])
 
     def lanes(where, size):
         return pl.ds(pl.multiple_of(where * size, size), size)
 
-    own = pltpu.make_async_copy(mixed_ref, heads.at[:, :, lanes(s, VAL)], own_sem)
-    own.start()
-    moves = [
-        pltpu.make_async_remote_copy(
-            src_ref=mixed_ref,
-            dst_ref=heads.at[:, :, lanes(s, VAL)],
-            send_sem=m_sem.at[0, k - 1],
-            recv_sem=m_sem.at[1, k - 1],
-            device_id=(g, z_at[k], t),
+    def remote(src, dst, sems, index, peer):
+        return pltpu.make_async_remote_copy(
+            src_ref=src,
+            dst_ref=dst,
+            send_sem=sems.at[(0, *index)],
+            recv_sem=sems.at[(1, *index)],
+            device_id=peer,
             device_id_type=MESH,
         )
-        for k in range(1, n_sp)
-    ]
-    for copy in moves:
-        copy.start()
-    own.wait()
-    for copy in moves:
-        copy.wait_recv()
-
-    def multiply(q, carry):
-        partial[q] = jnp.dot(
-            heads[q], w_ref[...], preferred_element_type=jnp.float32
-        ).astype(jnp.bfloat16)
+
+    w_rows = pl.ds(pl.multiple_of(c * depth, depth), depth)
+    w_own = pltpu.make_async_copy(w_ref.at[:, lanes(c, width)], matrix.at[w_rows, :], own_sem)
+    w_twin = remote(w_ref.at[:, lanes(1 - c, width)], matrix.at[w_rows, :], w_sem, (), (g, s, twin))
+    w_own.start()
+    w_twin.start()
+
+    def head(q, where):
+        return heads.at[q, :, lanes(c * n_sp + where, VAL)]
+
+    def slot(up, d):
+        return 1 + d if up else n_sp + d
+
+    def inside(place):
+        return jnp.logical_and(place >= 0, place < n_sp)
+
+    def z_move(q, up, d):
+        step = 1 if up else -1
+        here = head(q, s - step * d)
+        return remote(here, here, z_sem, (q, slot(up, d) - 1), (g, s + step, t))
+
+    def z_sends(up, d):
+        step = 1 if up else -1
+        return jnp.logical_and(inside(s + step), inside(s - step * d))
+
+    def z_gets(up, d):
+        step = 1 if up else -1
+        return inside(s - step * (d + 1))
+
+    def c_move(q, index, origin):
+        here = head(q, origin)
+        return remote(here, here, c_sem, (q, index), (g, s, twin))
+
+    def each(d, visit):
+        for up in (True, False):
+
+            @pl.when(z_gets(up, d))
+            def _():
+                visit(up, s - (d + 1) if up else s + (d + 1))
+
+    def arrived(q, d):
+        def visit(up, origin):
+            z_move(q, up, d).wait_recv()
+            if d + 1 < n_sp - 1:
+
+                @pl.when(z_sends(up, d + 1))
+                def _():
+                    z_move(q, up, d + 1).start()
+
+            c_move(q, slot(up, d), origin).start()
+
+        each(d, visit)
+
+    def advance(q, carry):
+        heads[q, :, lanes(c * n_sp + s, VAL)] = recur_one(
+            proj_ref, shift_ref, gap_ref, gain_ref, summed, q
+        )
+        for up in (True, False):
+
+            @pl.when(z_sends(up, 0))
+            def _():
+                z_move(q, up, 0).start()
+
+        c_move(q, 0, s).start()
+        for d in range(n_sp - 1):
+
+            @pl.when(q >= d + 1)
+            def _():
+                arrived(q - (d + 1), d)
+
         return carry
 
-    lax.fori_loop(0, seqs, multiply, 0)
+    lax.fori_loop(0, seqs, advance, 0)
 
     def piece(where_s, where_t):
         return pl.ds(pl.multiple_of((where_s * n_tp + where_t) * span, span), span)
 
-    sends = [
-        pltpu.make_async_remote_copy(
-            src_ref=partial.at[:, piece(z_at[k], t_at[j]), :],
-            dst_ref=landed.at[t, :, :, lanes(s, width)],
-            send_sem=p_sem.at[0, k, j],
-            recv_sem=p_sem.at[1, k, j],
-            device_id=(g, z_at[k], t_at[j]),
-            device_id_type=MESH,
-        )
-        for k, j in others
+    def p_move(h, k, j):
+        both = pl.ds(h * half, half)
+        return remote(
+            partial.at[both, piece(z_at[k], t_at[j]), :],
+            landed.at[x, both, :, lanes(s * CORES + c, width)],
+            p_sem,
+            (h, k, j),
+            (g, z_at[k], t_at[j]),
+        )
+
+    def finish(h):
+        def one(q, carry):
+            c_move(q, 0, s).wait_recv()
+            for d in range(n_sp - 1):
+                each(d, lambda up, origin: c_move(q, slot(up, d), origin).wait_recv())
+            partial[q] = jnp.dot(
+                heads[q], matrix[...], preferred_element_type=jnp.float32
+            ).astype(jnp.bfloat16)
+            return carry
+
+        lax.fori_loop(h * half, (h + 1) * half, one, 0)
+        for k, j in others:
+            p_move(h, k, j).start()
+        both = pl.ds(h * half, half)
+        landed[x, both, :, lanes(s * CORES + c, width)] = partial[both, piece(s, t), :]
+
+    w_own.wait()
+    w_twin.wait_recv()
+    pending = [
+        (i - 1 - d, d)
+        for i in range(seqs, seqs + n_sp - 1)
+        for d in range(n_sp - 1)
+        if 0 <= i - 1 - d < seqs
     ]
-    for copy in sends:
-        copy.start()
-    landed[t, :, :, lanes(s, width)] = partial[:, piece(s, t), :]
-    for copy in sends:
-        copy.wait_recv()
+    early = [item for item in pending if item[0] < half]
+    late = [item for item in pending if item[0] >= half]
+    cut = pending.index(early[-1]) + 1 if early else 0
+    for q, d in pending[:cut]:
+        arrived(q, d)
+    finish(0)
+    for q, d in pending[cut:]:
+        arrived(q, d)
+    finish(1)
+    for h in range(2):
+        for k, j in others:
+            p_move(h, k, j).wait_recv()
     total = landed[0].astype(jnp.float32)
-    for j in range(1, n_tp):
+    for j in range(1, n_x):
         total = total + landed[j].astype(jnp.float32)
     out_ref[...] = total.astype(jnp.bfloat16)
-    for copy in moves + sends:
-        copy.wait_send()
-
-
-def mix(sizes, mixed, w_out):
+
+    w_twin.wait_send()
+
+    def drain(q, carry):
+        c_move(q, 0, s).wait_send()
+        for d in range(n_sp - 1):
+            each(d, lambda up, origin: c_move(q, slot(up, d), origin).wait_send())
+            for up in (True, False):
+
+                @pl.when(z_sends(up, d))
+                def _():
+                    z_move(q, up, d).wait_send()
+
+        return carry
+
+    lax.fori_loop(0, seqs, drain, 0)
+    for h in range(2):
+        for k, j in others:
+            p_move(h, k, j).wait_send()
+
+
+def mix(sizes, proj, shift, gap, gain, w_out):
     n_grp, n_sp, n_tp = sizes
-    seqs, length, _ = mixed.shape
+    seqs, length, _ = proj.shape
     span = length // (n_sp * n_tp)
     depth, width = w_out.shape
+    part = width // CORES
     dma = pltpu.SemaphoreType.DMA
     vmem = pl.BlockSpec(memory_space=pltpu.VMEM)
     return pl.pallas_call(
         functools.partial(mix_kernel, sizes),
         out_shape=jax.ShapeDtypeStruct((seqs, span, n_sp * width), jnp.bfloat16),
-        in_specs=[pl.BlockSpec(memory_space=pltpu.HBM), vmem],
+        in_specs=[vmem, vmem, vmem, vmem, pl.BlockSpec(memory_space=pltpu.HBM)],
         out_specs=vmem,
         scratch_shapes=[
-            pltpu.VMEM((seqs, length, depth), jnp.bfloat16),
-            pltpu.VMEM((seqs, length, width), jnp.bfloat16),
-            pltpu.VMEM((n_tp, seqs, span, n_sp * width), jnp.bfloat16),
+            pltpu.VMEM((length, VAL), jnp.float32),
+            pltpu.VMEM((seqs, length, CORES * depth), jnp.bfloat16),
+            pltpu.VMEM((CORES * depth, part), jnp.bfloat16),
+            pltpu.VMEM((seqs, length, part), jnp.bfloat16),
+            pltpu.VMEM((n_tp // CORES, seqs, span, n_sp * width), jnp.bfloat16),
             dma,
-            dma((2, n_sp - 1)),
-            dma((2, n_sp, n_tp)),
+            dma((2,)),
+            dma((2, seqs, 2 * n_sp - 2)),
+            dma((2, seqs, 2 * n_sp - 1)),
+            dma((2, 2, n_sp, n_tp)),
         ],
         compiler_params=pltpu.CompilerParams(collective_id=1, has_side_effects=True),
-    )(mixed, w_out)
+    )(proj, shift, gap, gain, w_out)
 
 
 def head_shards(
@@ -607,13 +799,12 @@
     proj, shift = gather_project(
         sizes,
         normed.transpose(1, 0, 2),
-        decay_shift.transpose(1, 0, 2),
+        decay_shift.astype(jnp.bfloat16).transpose(1, 0, 2),
         (w_query, w_value, w_fwd_gate, w_bwd_gate, w_out_gate),
     )
     first = lax.axis_index("sp") * KEY
     gap = lax.dynamic_slice_in_dim(floor_gap, first, KEY, axis=1)
-    mixed = recur(proj, shift, gap, head_gain.reshape(1, VAL))
-    return mix(sizes, mixed, w_out).transpose(1, 0, 2)
+    return mix(sizes, proj, shift, gap, head_gain.reshape(1, VAL), w_out).transpose(1, 0, 2)
 
 
 def by_heads(mesh):
@@ -625,6 +816,7 @@
         span = tokens.shape[0] // (n_sp * n_tp)
         sizes = (mesh.shape["grp"], n_sp, n_tp)
         fits = heads_here == n_sp and n_sp > 1 and n_tp % CORES == 0 and span % 16 == 0
+        fits = fits and tokens.shape[1] // sizes[0] % 2 == 0
         fits = fits and tokens.shape[0] % BLOCK == 0 and tokens.shape[0] <= 512
         body = functools.partial(head_shards, sizes) if fits else shards
         return mapped(body, mesh)(*arrays)

time: 151 us -> 114 us (0.75)
  Pallas kernels: 143 us -> 105 us
    pallas_call x1, Pallas kernels: 76 us -> 53.2 us  [gather_project(): pl.pallas_call(functools.partial(gather_kernel, sizes), out_shape=(jax.Sh...]
    pallas_call x1 -> x0, Pallas kernels: 10.7 us -> none  [recur(): pl.pallas_call(recur_kernel, grid=(seqs,), out_shape=jax.ShapeDtypeStruct...]
    pallas_call x1, Pallas kernels: 56.1 us -> 52.2 us  [mix(): pl.pallas_call(functools.partial(mix_kernel, sizes), out_shape=jax.ShapeD...]
where the time goes in v2:
time: 114 us; the launch traced here: 113 us
  Pallas kernels  105 us (92%)
  local copies, waits for them, and re-layouts  4.32 us (4%)
  other arithmetic  3.11 us (3%)
    pallas_call x1, Pallas kernels, gather_project(): pl.pallas_call(functools.partial(gather_kernel, sizes), out_shape=(jax.Sh...  53.2 us
    pallas_call x1, Pallas kernels, mix(): pl.pallas_call(functools.partial(mix_kernel, sizes), out_shape=jax.ShapeD...  52.2 us

profile of v2, /device:TPU:25, one launch (start us, length us, event | category | flops | bytes accessed | tf_op | source)
XLA Modules:
  0.0 112.9 jit_solution(12255636785399236551)
XLA Ops:
  0.0 0.0 copy-start
  0.0 1.2 %fusion = f32[16,4]{0,1:T(4,128)S(1)} fusion(bf16[16,4,2048]{2,1,0:T(4,128)(2,1)} %param.11), kind=kLoop, calls=%fused_computation.2 | loop fusion | flops 393152 | bytes 262400 | tf_op jit(solution)/shard_map/reduce_sum | solution.py:797
  1.2 1.9 %fusion.4.xn_ref = bf16[4,16,2048]{2,1,0:T(8,128)(2,1)} fusion(f32[2048]{0:T(1024)} %param.12, f32[16,4]{0,1:T(4,128)S(1)} %add_rsqrt_fusion, bf16[16,4,2048]{2,1,0:T(4,128)(2,1)} %param.11), kind=kLoop, calls=%fused_computation.7 | loop fusion | flops 524288 | bytes 532736 | tf_op jit(solution)/shard_map/transpose | solution.py:801
  3.1 1.9 %copy.20 = bf16[64,4,512]{2,0,1:T(8,128)(2,1)} copy(f32[64,4,512]{2,1,0:T(4,128)} %param.19) | data formatting | bytes 786432 | tf_op args[8]
  5.0 53.2 %shard_map.109 = (bf16[4,256,640]{2,1,0:T(8,128)(2,1)}, bf16[4,256,128]{2,1,0:T(8,128)(2,1)}) custom-call(bf16[4,16,2048]{2,1,0:T(8,128)(2,1)} %fusion.4.xn_ref, bf16[4,64,512]{2,1,0:T(8,128)(2,1)} %bitcast.7, bf16[512,512]{1,0:T(8,128)(2,1)} %wq_ref.1, bf16[512,512]{1,0:T(8,128)(2,1)} %wv_ref.1, bf16[512,512]{1,0:T(8,128)(2,1)} %wf_ref.1, ...), custom_call_target="tpu_custom_call" | custom-call | tf_op jit(solution)/shard_map/pallas_call | solution.py:470
  58.2 0.0 copy-done
  58.2 0.6 constant_dynamic-slice_fusion.gap_ref
  58.8 52.2 %shard_map.110 = bf16[4,16,2048]{2,1,0:T(8,128)(2,1)} custom-call(bf16[4,256,640]{2,1,0:T(8,128)(2,1)} %get-tuple-element.7.proj_ref, bf16[4,256,128]{2,1,0:T(8,128)(2,1)} %get-tuple-element.8.shift_ref, f32[2,128]{1,0:T(2,128)} %constant_dynamic-slice_fusion.gap_ref, f32[1,128]{1,0:T(1,128)} %bitcast.9, bf16[512,512]{1,0:T(8,128)(2,1)} %w_ref.1), custom_call_target="tpu_custom_call" | custom-call | tf_op jit(solution)/shard_map/pallas_call | solution.py:761
  111.1 1.9 %copy.14 = bf16[16,4,2048]{2,1,0:T(4,128)(2,1)} copy(bf16[16,4,2048]{2,0,1:T(8,128)(2,1)} %bitcast.8) | data formatting | bytes 524288 | tf_op jit(solution)/shard_map/transpose | solution.py:807
  (1 shorter events, 0.0 us)
Async XLA Ops:
  0.0 58.2 %copy-start = (f32[2,512]{1,0:T(2,128)S(1)}, f32[2,512]{1,0:T(2,128)}, u32[]{:S(2)}) copy-start(f32[2,512]{1,0:T(2,128)} %param.18) | copy-start | bytes 12292

commit v3 on v2

--- a/solution.py
+++ b/solution.py
@@ -213,7 +213,7 @@
     pl.semaphore_wait(barrier, len(peers))
 
 
-def gather_kernel(
+def gather_phase(
     sizes,
     xn_ref,
     shift_ref,
@@ -223,7 +223,6 @@
     wb_ref,
     wg_ref,
     proj_ref,
-    shift_out_ref,
     acts,
     weights,
     shifts,
@@ -256,12 +255,6 @@
     y_at = [g] + [lax.rem(g + m, n_grp) for m in range(1, n_grp)]
     y_from = [g] + [lax.rem(g + n_grp - m, n_grp) for m in range(1, n_grp)]
 
-    peers = [(g, z_at[k], t) for k in range(1, n_sp)]
-    peers += [(g, s, x_at[j]) for j in range(1, n_x)]
-    peers += [(g, s, twin)]
-    peers += [(y_at[m], s, t) for m in range(1, n_grp)]
-    greet(peers)
-
     def block(where_s, where_t):
         return acts.at[:, pl.ds(pl.multiple_of((where_s * n_tp + where_t) * span, span), span), :]
 
@@ -356,6 +349,15 @@
                 )
             )
 
+    w_y = {}
+
+    def swap(p):
+        for k in range(1, n_sp):
+            w_z[k, p].wait_recv()
+            here = weights.at[rows(z_from[k], g), pl.ds(p * KEY, KEY)]
+            for m in range(1, n_grp):
+                w_y[m, k, p] = go(remote(here, here, wy_sem, (m - 1, k - 1, p), (y_at[m], s, t)))
+
     queue = list(range(len(sources)))
     for d in range(n_sp - 1):
         if queue:
@@ -377,8 +379,13 @@
                     act_spread("x", j, slot(up, d), origin, t, False).start()
                 act_spread("c", 0, slot(up, d), origin, t, False).start()
 
-    for p in queue:
-        send_weights(p)
+        if d == n_sp - 2:
+            for p in queue:
+                send_weights(p)
+            queue = []
+        if d >= 1:
+            swap(d - 1)
+
     s_z = {}
     for k in range(1, n_sp):
         s_z[k] = go(
@@ -391,9 +398,10 @@
             )
         )
 
-    def each_block(visit):
-        visit(0, s)
-        for d in range(n_sp - 1):
+    def each_block(visit, ds=None):
+        if ds is None:
+            visit(0, s)
+        for d in range(n_sp - 1) if ds is None else ds:
             for up in (True, False):
                 _, _, _, origin, gets = chain(up, d)
 
@@ -406,14 +414,14 @@
             act_spread("x", j, index, origin, t, False).wait_recv()
             act_spread("c", j, index, origin, x_from[j], False).start()
 
-    each_block(relay)
-    w_y = {}
-    for p in range(len(sources)):
-        for k in range(1, n_sp):
-            w_z[k, p].wait_recv()
-            here = weights.at[rows(z_from[k], g), pl.ds(p * KEY, KEY)]
-            for m in range(1, n_grp):
-                w_y[m, k, p] = go(remote(here, here, wy_sem, (m - 1, k - 1, p), (y_at[m], s, t)))
+    relay(0, s)
+    left = list(range(max(n_sp - 2, 0), len(sources)))
+    for d in range(n_sp - 1):
+        each_block(relay, [d])
+        if left:
+            swap(left.pop(0))
+    for p in left:
+        swap(p)
     for copy in mine:
         copy.wait()
 
@@ -438,7 +446,6 @@
         lax.fori_loop(0, seqs, project, 0)
     for copy in s_z.values():
         copy.wait_recv()
-    shift_out_ref[...] = shifts[...]
     for d in range(n_sp - 1):
         for up in (True, False):
             _, _, sends, _, _ = chain(up, d)
@@ -458,42 +465,7 @@
         copy.wait_send()
 
 
-def gather_project(sizes, xn, shift, sources):
-    n_grp, n_sp, n_tp = sizes
-    n_x = n_tp // CORES
-    seqs, span, model = xn.shape
-    length = n_sp * n_tp * span
-    width = len(sources) * KEY
-    dma = pltpu.SemaphoreType.DMA
-    hbm = pl.BlockSpec(memory_space=pltpu.HBM)
-    vmem = pl.BlockSpec(memory_space=pltpu.VMEM)
-    return pl.pallas_call(
-        functools.partial(gather_kernel, sizes),
-        out_shape=(
-            jax.ShapeDtypeStruct((seqs, length, width), jnp.bfloat16),
-            jax.ShapeDtypeStruct((seqs, length, KEY), shift.dtype),
-        ),
-        in_specs=[hbm] * (2 + len(sources)),
-        out_specs=(vmem, vmem),
-        scratch_shapes=[
-            pltpu.VMEM((seqs, length, model), jnp.bfloat16),
-            pltpu.VMEM((model, width), jnp.bfloat16),
-            pltpu.VMEM((seqs, length, KEY), shift.dtype),
-            dma((len(sources) + 2,)),
-            dma((2, 2 * n_sp - 2)),
-            dma((2, max(n_x - 1, 1), 2 * n_sp - 1)),
-            dma((2, n_x, 2 * n_sp - 1)),
-            dma((2, n_sp - 1, len(sources))),
-            dma((2, max(n_grp - 1, 1), n_sp - 1, len(sources))),
-            dma((2, n_sp - 1)),
-        ],
-        compiler_params=pltpu.CompilerParams(
-            collective_id=0, has_side_effects=True, vmem_limit_bytes=56 * 1024 * 1024
-        ),
-    )(xn, shift, *sources)
-
-
-def recur_one(proj_ref, shift_ref, gap_ref, gain_ref, out_ref, i):
+def recur_one(proj_ref, shift_ref, gap_ref, gain_ref, out_ref, i, own):
     f32 = jnp.float32
     bf16 = jnp.bfloat16
     length = proj_ref.shape[1]
@@ -505,56 +477,71 @@
     queries = queries * jax.nn.sigmoid(queries)
     values = cols(1)
     shift = shift_ref[i].astype(f32)
+    row = lax.broadcasted_iota(jnp.int32, (length, length), 0)
+    col = lax.broadcasted_iota(jnp.int32, (length, length), 1)
+    near = row // BLOCK == col // BLOCK
     row = lax.broadcasted_iota(jnp.int32, (BLOCK, BLOCK), 0)
-    col = lax.broadcasted_iota(jnp.int32, (BLOCK, BLOCK), 1)
+    col_b = lax.broadcasted_iota(jnp.int32, (BLOCK, BLOCK), 1)
+    seen = [row >= col_b, row <= col_b]
+    row_l = lax.broadcasted_iota(jnp.int32, (length, length), 0)
+    order = [row_l >= col, row_l <= col]
     blocks = length // BLOCK
+    keys, here = [], []
     for d in range(2):
-        keys = gap_ref[d : d + 1, :] * jax.nn.sigmoid(-cols(2 + d).astype(f32))
-        decay = jnp.log1p(-keys) + shift
-        seen = (row >= col) if d == 0 else (row <= col)
-        tri = jnp.where(seen, 1.0, 0.0).astype(f32)
-        state = None
-        for step in range(blocks):
+        key = gap_ref[d : d + 1, own] * jax.nn.sigmoid(-cols(2 + d).astype(f32))
+        decay = jnp.log1p(-key) + shift
+        high = decay.astype(bf16)
+        rest = decay - high.astype(f32)
+        middle = rest.astype(bf16)
+        low = (rest - middle.astype(f32)).astype(bf16)
+        tri = jnp.where(jnp.logical_and(near, order[d]), 1.0, 0.0).astype(bf16)
+        sums = jnp.dot(
+            tri, jnp.concatenate([high, middle, low], axis=1), preferred_element_type=f32
+        )
+        here.append(sums[:, :KEY] + (sums[:, KEY : 2 * KEY] + sums[:, 2 * KEY :]))
+        keys.append(key)
+    state = [None, None]
+    outs = [[None, None] for _ in range(blocks)]
+    for step in range(blocks):
+        for d in range(2):
             n = step if d == 0 else blocks - 1 - step
             at = slice(n * BLOCK, (n + 1) * BLOCK)
-            q, k, v = queries[at], keys[at], values[at]
-            here = jnp.dot(tri, decay[at], precision=highest, preferred_element_type=f32)
-            edge = here[BLOCK - 1 : BLOCK] if d == 0 else here[0:1]
-            anchor = here[BLOCK // 2 : BLOCK // 2 + 1]
+            q, k, v, h = queries[at], keys[d][at], values[at], here[d][at]
+            edge = h[BLOCK - 1 : BLOCK] if d == 0 else h[0:1]
+            anchor = h[BLOCK // 2 : BLOCK // 2 + 1]
             scores = lax.dot_general(
-                (q * jnp.exp(here - anchor)).astype(bf16),
-                (k * jnp.exp(anchor - here)).astype(bf16),
+                (q * jnp.exp(h - anchor)).astype(bf16),
+                (k * jnp.exp(anchor - h)).astype(bf16),
                 (((1,), (1,)), ((), ())),
                 preferred_element_type=f32,
             )
-            scores = jnp.where(seen, scores, 0.0).astype(bf16)
+            scores = jnp.where(seen[d], scores, 0.0).astype(bf16)
             out = jnp.dot(scores, v, preferred_element_type=f32)
-            if state is not None:
+            if state[d] is not None:
                 out = out + lax.dot_general(
-                    (q * jnp.exp(here)).astype(bf16),
-                    state.astype(bf16),
+                    (q * jnp.exp(h)).astype(bf16),
+                    state[d].astype(bf16),
                     (((1,), (1,)), ((), ())),
                     preferred_element_type=f32,
                 )
-            if d == 0:
-                out_ref[at] = out
-            else:
-                out_ref[at] = out_ref[at] + out
+            outs[n][d] = out
             if step < blocks - 1:
                 fresh = lax.dot_general(
                     v,
-                    (k * jnp.exp(edge - here)).astype(bf16),
+                    (k * jnp.exp(edge - h)).astype(bf16),
                     (((0,), (0,)), ((), ())),
                     preferred_element_type=f32,
                 )
-                state = fresh if state is None else state * jnp.exp(edge) + fresh
+                state[d] = fresh if state[d] is None else state[d] * jnp.exp(edge) + fresh
+    for n in range(blocks):
+        out_ref[n * BLOCK : (n + 1) * BLOCK] = outs[n][0] + outs[n][1]
     combined = out_ref[...]
     normed = combined * lax.rsqrt(jnp.mean(combined * combined, axis=-1, keepdims=True) + norm_eps)
     gate = cols(4).astype(f32)
     return (normed * gain_ref[...] * (gate * jax.nn.sigmoid(gate))).astype(bf16)
 
 
-def mix_kernel(
+def mix_phase(
     sizes,
     proj_ref,
     shift_ref,
@@ -588,7 +575,6 @@
     z_at = [lax.rem(s + k, n_sp) for k in range(n_sp)]
     t_at = [lax.rem(t + j, n_tp) for j in range(n_tp)]
     others = [(k, j) for k in range(n_sp) for j in range(n_tp) if k or j]
-    greet([(g, z_at[k], t_at[j]) for k, j in others])
 
     def lanes(where, size):
         return pl.ds(pl.multiple_of(where * size, size), size)
@@ -657,7 +643,7 @@
 
     def advance(q, carry):
         heads[q, :, lanes(c * n_sp + s, VAL)] = recur_one(
-            proj_ref, shift_ref, gap_ref, gain_ref, summed, q
+            proj_ref, shift_ref, gap_ref, gain_ref, summed, q, lanes(s, KEY)
         )
         for up in (True, False):
 
@@ -750,33 +736,138 @@
             p_move(h, k, j).wait_send()
 
 
-def mix(sizes, proj, shift, gap, gain, w_out):
+def layer_kernel(
+    sizes,
+    xn_ref,
+    shift_ref,
+    wq_ref,
+    wv_ref,
+    wf_ref,
+    wb_ref,
+    wg_ref,
+    gap_ref,
+    gain_ref,
+    w_ref,
+    out_ref,
+    proj,
+    acts,
+    weights,
+    shifts,
+    summed,
+    heads,
+    matrix,
+    partial,
+    landed,
+    own_sem,
+    az_sem,
+    ax_sem,
+    ac_sem,
+    wz_sem,
+    wy_sem,
+    sz_sem,
+    mix_own_sem,
+    mix_w_sem,
+    mix_z_sem,
+    mix_c_sem,
+    mix_p_sem,
+):
     n_grp, n_sp, n_tp = sizes
-    seqs, length, _ = proj.shape
-    span = length // (n_sp * n_tp)
+    g = lax.axis_index("grp")
+    s = lax.axis_index("sp")
+    t = lax.axis_index("tp")
+    peers = [
+        (g, lax.rem(s + k, n_sp), lax.rem(t + j, n_tp))
+        for k in range(n_sp)
+        for j in range(n_tp)
+        if k or j
+    ]
+    peers += [(lax.rem(g + m, n_grp), s, t) for m in range(1, n_grp)]
+    greet(peers)
+    gather_phase(
+        sizes,
+        xn_ref,
+        shift_ref,
+        wq_ref,
+        wv_ref,
+        wf_ref,
+        wb_ref,
+        wg_ref,
+        proj,
+        acts,
+        weights,
+        shifts,
+        own_sem,
+        az_sem,
+        ax_sem,
+        ac_sem,
+        wz_sem,
+        wy_sem,
+        sz_sem,
+    )
+    mix_phase(
+        sizes,
+        proj,
+        shifts,
+        gap_ref,
+        gain_ref,
+        w_ref,
+        out_ref,
+        summed,
+        heads,
+        matrix,
+        partial,
+        landed,
+        mix_own_sem,
+        mix_w_sem,
+        mix_z_sem,
+        mix_c_sem,
+        mix_p_sem,
+    )
+
+
+def layer(sizes, xn, shift, sources, gap, gain, w_out):
+    n_grp, n_sp, n_tp = sizes
+    n_x = n_tp // CORES
+    seqs, span, model = xn.shape
+    length = n_sp * n_tp * span
+    count = len(sources)
     depth, width = w_out.shape
     part = width // CORES
     dma = pltpu.SemaphoreType.DMA
+    hbm = pl.BlockSpec(memory_space=pltpu.HBM)
     vmem = pl.BlockSpec(memory_space=pltpu.VMEM)
     return pl.pallas_call(
-        functools.partial(mix_kernel, sizes),
+        functools.partial(layer_kernel, sizes),
         out_shape=jax.ShapeDtypeStruct((seqs, span, n_sp * width), jnp.bfloat16),
-        in_specs=[vmem, vmem, vmem, vmem, pl.BlockSpec(memory_space=pltpu.HBM)],
+        in_specs=[hbm] * (2 + count) + [vmem, vmem, hbm],
         out_specs=vmem,
         scratch_shapes=[
+            pltpu.VMEM((seqs, length, count * KEY), jnp.bfloat16),
+            pltpu.VMEM((seqs, length, model), jnp.bfloat16),
+            pltpu.VMEM((model, count * KEY), jnp.bfloat16),
+            pltpu.VMEM((seqs, length, KEY), shift.dtype),
             pltpu.VMEM((length, VAL), jnp.float32),
             pltpu.VMEM((seqs, length, CORES * depth), jnp.bfloat16),
             pltpu.VMEM((CORES * depth, part), jnp.bfloat16),
             pltpu.VMEM((seqs, length, part), jnp.bfloat16),
-            pltpu.VMEM((n_tp // CORES, seqs, span, n_sp * width), jnp.bfloat16),
+            pltpu.VMEM((n_x, seqs, span, n_sp * width), jnp.bfloat16),
+            dma((count + 2,)),
+            dma((2, 2 * n_sp - 2)),
+            dma((2, max(n_x - 1, 1), 2 * n_sp - 1)),
+            dma((2, n_x, 2 * n_sp - 1)),
+            dma((2, n_sp - 1, count)),
+            dma((2, max(n_grp - 1, 1), n_sp - 1, count)),
+            dma((2, n_sp - 1)),
             dma,
             dma((2,)),
             dma((2, seqs, 2 * n_sp - 2)),
             dma((2, seqs, 2 * n_sp - 1)),
             dma((2, 2, n_sp, n_tp)),
         ],
-        compiler_params=pltpu.CompilerParams(collective_id=1, has_side_effects=True),
-    )(proj, shift, gap, gain, w_out)
+        compiler_params=pltpu.CompilerParams(
+            collective_id=0, has_side_effects=True, vmem_limit_bytes=56 * 1024 * 1024
+        ),
+    )(xn, shift, *sources, gap, gain, w_out)
 
 
 def head_shards(
@@ -796,15 +887,15 @@
     token_f32 = tokens.astype(jnp.float32)
     scale_rows = lax.rsqrt(jnp.mean(token_f32 * token_f32, axis=-1, keepdims=True) + norm_eps)
     normed = (token_f32 * scale_rows * norm_gain).astype(jnp.bfloat16)
-    proj, shift = gather_project(
+    return layer(
         sizes,
         normed.transpose(1, 0, 2),
         decay_shift.astype(jnp.bfloat16).transpose(1, 0, 2),
         (w_query, w_value, w_fwd_gate, w_bwd_gate, w_out_gate),
-    )
-    first = lax.axis_index("sp") * KEY
-    gap = lax.dynamic_slice_in_dim(floor_gap, first, KEY, axis=1)
-    return mix(sizes, proj, shift, gap, head_gain.reshape(1, VAL), w_out).transpose(1, 0, 2)
+        floor_gap,
+        head_gain.reshape(1, VAL),
+        w_out,
+    ).transpose(1, 0, 2)
 
 
 def by_heads(mesh):

time: 114 us -> 99.6 us (0.87)
  Pallas kernels: 105 us -> 93.2 us
  local copies, waits for them, and re-layouts: 4.32 us -> 2.72 us
    pallas_call x2 -> x1, Pallas kernels: 105 us -> 93.2 us  [layer(): pl.pallas_call(functools.partial(layer_kernel, sizes), out_shape=jax.Shap...]
where the time goes in v3:
time: 99.6 us; the launch traced here: 98.9 us
  Pallas kernels  93.2 us (94%)
  other arithmetic  2.88 us (3%)
  local copies, waits for them, and re-layouts  2.72 us (3%)
    pallas_call x1, Pallas kernels, layer(): pl.pallas_call(functools.partial(layer_kernel, sizes), out_shape=jax.Shap...  93.2 us

profile of v3, /device:TPU:25, one launch (start us, length us, event | category | flops | bytes accessed | tf_op | source)
XLA Modules:
  0.0 98.9 jit_solution(13043015957334732877)
XLA Ops:
  0.0 0.0 copy-start
  0.0 0.0 copy-start.1
  0.0 1.3 %fusion = f32[16,4]{0,1:T(4,128)S(1)} fusion(bf16[16,4,2048]{2,1,0:T(4,128)(2,1)} %param.11), kind=kLoop, calls=%fused_computation.2 | loop fusion | flops 393152 | bytes 262400 | tf_op jit(solution)/shard_map/reduce_sum | solution.py:888
  1.3 0.0 copy-done
  1.3 1.6 %fusion.4.xn_ref = bf16[4,16,2048]{2,1,0:T(8,128)(2,1)} fusion(f32[2048]{0:T(1024)} %param.12, f32[16,4]{0,1:T(4,128)S(1)} %add_rsqrt_fusion, bf16[16,4,2048]{2,1,0:T(4,128)(2,1)S(1)} %copy-done), kind=kLoop, calls=%fused_computation.7 | loop fusion | flops 524288 | bytes 532736 | tf_op jit(solution)/shard_map/transpose | solution.py:892
  2.9 0.0 copy-done.1
  2.9 0.8 copy.20
  3.8 93.2 %shard_map.109 = bf16[4,16,2048]{2,1,0:T(8,128)(2,1)} custom-call(bf16[4,16,2048]{2,1,0:T(8,128)(2,1)} %fusion.4.xn_ref, bf16[4,64,512]{2,1,0:T(8,128)(2,1)} %bitcast.7, bf16[512,512]{1,0:T(8,128)(2,1)} %wq_ref.1, bf16[512,512]{1,0:T(8,128)(2,1)} %wv_ref.1, bf16[512,512]{1,0:T(8,128)(2,1)} %wf_ref.1, bf16[512,512]{1,0:T(8,128)(2,1)} %wb_ref.1, ...), custom_call_target="tpu_custom_call" | custom-call | tf_op jit(solution)/shard_map/pallas_call | solution.py:839
  97.0 1.9 %copy.14 = bf16[16,4,2048]{2,1,0:T(4,128)(2,1)} copy(bf16[16,4,2048]{2,0,1:T(8,128)(2,1)} %bitcast.8) | data formatting | bytes 524288 | tf_op jit(solution)/shard_map/transpose | solution.py:898
  (1 shorter events, 0.0 us)
Async XLA Ops:
  0.0 1.3 %copy-start = (bf16[16,4,2048]{2,1,0:T(4,128)(2,1)S(1)}, bf16[16,4,2048]{2,1,0:T(4,128)(2,1)}, u32[]{:S(2)}) copy-start(bf16[16,4,2048]{2,1,0:T(4,128)(2,1)} %param.11) | copy-start | bytes 786436
  0.0 2.9 %copy-start.1 = (f32[64,4,512]{2,1,0:T(4,128)S(1)}, f32[64,4,512]{2,1,0:T(4,128)}, u32[]{:S(2)}) copy-start(f32[64,4,512]{2,1,0:T(4,128)} %param.19) | copy-start | bytes 1572868

commit v4 on v3

--- a/solution.py
+++ b/solution.py
@@ -282,12 +282,11 @@
         )
         for p, w in enumerate(sources)
     ]
-    mine.append(pltpu.make_async_copy(xn_ref, block(s, t), own_sem.at[len(sources)]))
     mine.append(
         pltpu.make_async_copy(
             shift_ref.at[:, :, lanes(s)],
             shifts.at[:, pl.ds(pl.multiple_of(s * positions, positions), positions), :],
-            own_sem.at[len(sources) + 1],
+            own_sem.at[len(sources)],
         )
     )
 
@@ -313,11 +312,11 @@
 
     def act_move(up, d, from_own):
         there, origin, _, _, _ = chain(up, d)
-        src = xn_ref if from_own else block(origin, t)
+        src = block(origin, t)
         return remote(src, block(origin, t), az_sem, (slot(up, d) - 1,), (g, there, t))
 
     def act_spread(kind, j, index, where_s, where_t, from_own):
-        src = xn_ref if from_own else block(where_s, where_t)
+        src = block(where_s, where_t)
         if kind == "x":
             return remote(src, block(where_s, where_t), ax_sem, (j - 1, index), (g, s, x_at[j]))
         return remote(src, block(where_s, where_t), ac_sem, (j, index), (g, s, twin))
@@ -360,7 +359,7 @@
 
     queue = list(range(len(sources)))
     for d in range(n_sp - 1):
-        if queue:
+        if queue and d >= 1:
             send_weights(queue.pop(0))
         for up in (True, False):
             _, _, _, origin, gets = chain(up, d)
@@ -383,8 +382,8 @@
             for p in queue:
                 send_weights(p)
             queue = []
-        if d >= 1:
-            swap(d - 1)
+        if d >= 2:
+            swap(d - 2)
 
     s_z = {}
     for k in range(1, n_sp):
@@ -415,7 +414,7 @@
             act_spread("c", j, index, origin, x_from[j], False).start()
 
     relay(0, s)
-    left = list(range(max(n_sp - 2, 0), len(sources)))
+    left = list(range(max(n_sp - 3, 0), len(sources)))
     for d in range(n_sp - 1):
         each_block(relay, [d])
         if left:
@@ -739,6 +738,7 @@
 def layer_kernel(
     sizes,
     xn_ref,
+    norm_ref,
     shift_ref,
     wq_ref,
     wv_ref,
@@ -782,6 +782,12 @@
         if k or j
     ]
     peers += [(lax.rem(g + m, n_grp), s, t) for m in range(1, n_grp)]
+    span = xn_ref.shape[1]
+    rows = xn_ref[...].astype(jnp.float32)
+    scale = lax.rsqrt(jnp.mean(rows * rows, axis=-1, keepdims=True) + norm_eps)
+    acts[:, pl.ds(pl.multiple_of((s * n_tp + t) * span, span), span), :] = (
+        rows * scale * norm_ref[...]
+    ).astype(jnp.bfloat16)
     greet(peers)
     gather_phase(
         sizes,
@@ -825,7 +831,7 @@
     )
 
 
-def layer(sizes, xn, shift, sources, gap, gain, w_out):
+def layer(sizes, xn, norm_gain, shift, sources, gap, gain, w_out):
     n_grp, n_sp, n_tp = sizes
     n_x = n_tp // CORES
     seqs, span, model = xn.shape
@@ -839,7 +845,7 @@
     return pl.pallas_call(
         functools.partial(layer_kernel, sizes),
         out_shape=jax.ShapeDtypeStruct((seqs, span, n_sp * width), jnp.bfloat16),
-        in_specs=[hbm] * (2 + count) + [vmem, vmem, hbm],
+        in_specs=[vmem, vmem] + [hbm] * (1 + count) + [vmem, vmem, hbm],
         out_specs=vmem,
         scratch_shapes=[
             pltpu.VMEM((seqs, length, count * KEY), jnp.bfloat16),
@@ -851,7 +857,7 @@
             pltpu.VMEM((CORES * depth, part), jnp.bfloat16),
             pltpu.VMEM((seqs, length, part), jnp.bfloat16),
             pltpu.VMEM((n_x, seqs, span, n_sp * width), jnp.bfloat16),
-            dma((count + 2,)),
+            dma((count + 1,)),
             dma((2, 2 * n_sp - 2)),
             dma((2, max(n_x - 1, 1), 2 * n_sp - 1)),
             dma((2, n_x, 2 * n_sp - 1)),
@@ -867,7 +873,7 @@
         compiler_params=pltpu.CompilerParams(
             collective_id=0, has_side_effects=True, vmem_limit_bytes=56 * 1024 * 1024
         ),
-    )(xn, shift, *sources, gap, gain, w_out)
+    )(xn, norm_gain, shift, *sources, gap, gain, w_out)
 
 
 def head_shards(
@@ -884,12 +890,10 @@
     head_gain,
     w_out,
 ):
-    token_f32 = tokens.astype(jnp.float32)
-    scale_rows = lax.rsqrt(jnp.mean(token_f32 * token_f32, axis=-1, keepdims=True) + norm_eps)
-    normed = (token_f32 * scale_rows * norm_gain).astype(jnp.bfloat16)
     return layer(
         sizes,
-        normed.transpose(1, 0, 2),
+        tokens.transpose(1, 0, 2),
+        norm_gain.reshape(1, 1, -1),
         decay_shift.astype(jnp.bfloat16).transpose(1, 0, 2),
         (w_query, w_value, w_fwd_gate, w_bwd_gate, w_out_gate),
         floor_gap,

time: 99.6 us -> 95.7 us (0.961)
  Pallas kernels: 93.2 us -> 90.2 us
  other arithmetic: 2.88 us -> 0 us
  local copies, waits for them, and re-layouts: 2.72 us -> 4.56 us
    pallas_call x1, Pallas kernels: 93.2 us -> 90.2 us  [layer(): pl.pallas_call(functools.partial(layer_kernel, sizes), out_shape=jax.Shap...]
    unnamed x5 -> x4, local copies, waits for them, and re-layouts: 0.86 us -> 2.7 us
    transpose x1 -> x0, other arithmetic: 1.58 us -> none  [head_shards(): normed.transpose(1, 0, 2)]
    reduce_sum x1 -> x0, other arithmetic: 1.28 us -> none  [head_shards(): jnp.mean(token_f32 * token_f32, axis=-1, keepdims=True) + norm_eps]
where the time goes in v4:
time: 95.7 us; the launch traced here: 94.8 us
  Pallas kernels  90.2 us (94%)
  local copies, waits for them, and re-layouts  4.56 us (5%)
    pallas_call x1, Pallas kernels, layer(): pl.pallas_call(functools.partial(layer_kernel, sizes), out_shape=jax.Shap...  90.2 us
    unnamed x4, local copies, waits for them, and re-layouts  2.7 us

profile of v4, /device:TPU:25, one launch (start us, length us, event | category | flops | bytes accessed | tf_op | source)
XLA Modules:
  0.0 94.8 jit_solution(10452576126806556290)
XLA Ops:
  0.0 0.0 copy-start
  0.0 1.9 %copy.20 = bf16[16,4,2048]{2,0,1:T(8,128)(2,1)} copy(bf16[16,4,2048]{2,1,0:T(4,128)(2,1)} %param.11) | data formatting | bytes 524288 | tf_op args[0]
  1.9 0.0 copy-done
  1.9 0.8 copy.19
  2.7 90.2 %shard_map.109 = bf16[4,16,2048]{2,1,0:T(8,128)(2,1)} custom-call(bf16[4,16,2048]{2,1,0:T(8,128)(2,1)} %bitcast.11, f32[1,1,2048]{2,1,0:T(1,128)} %bitcast.12, bf16[4,64,512]{2,1,0:T(8,128)(2,1)} %bitcast.9, bf16[512,512]{1,0:T(8,128)(2,1)} %wq_ref.1, bf16[512,512]{1,0:T(8,128)(2,1)} %wv_ref.1, bf16[512,512]{1,0:T(8,128)(2,1)} %wf_ref.1, ...), custom_call_target="tpu_custom_call" | custom-call | tf_op jit(solution)/shard_map/pallas_call | solution.py:845
  92.9 1.9 %copy.14 = bf16[16,4,2048]{2,1,0:T(4,128)(2,1)} copy(bf16[16,4,2048]{2,0,1:T(8,128)(2,1)} %bitcast.10) | data formatting | bytes 524288 | tf_op jit(solution)/shard_map/transpose | solution.py:902
Async XLA Ops:
  0.0 1.9 %copy-start = (f32[64,4,512]{2,1,0:T(4,128)S(1)}, f32[64,4,512]{2,1,0:T(4,128)}, u32[]{:S(2)}) copy-start(f32[64,4,512]{2,1,0:T(4,128)} %param.19) | copy-start | bytes 1572868
